TPU v7x, 128 devices: a whole 4x4x4 slice. The times are simulated.
128 devices in a mesh: sp: 32 (over z, y, core), tp: 4 (over x).
Axes of the slice: x: 4, y: 4, z: 4, core: 2. Of those that a mesh axis runs over, the one named last changes fastest.
Arguments:
- moe_input: bfloat16 [8192, 2048], P('sp'), may hold values from -17.5 to 17.5
- cotangent: bfloat16 [8192, 2048], P('sp'), may hold values from -6 to 6
- routes: int32 [8192, 2], P('sp'), may hold values from 0 to 31, all different within a row; in each aligned block of 256 rows (0 to 255, 256 to 511, ...) at most 20 rows name the same one
- route_weights: float32 [8192, 2], P('sp'), may hold values from 0.2 to 1
- gate_weight: bfloat16 [32, 2048, 2048], P('sp', None, 'tp'), may hold values from -0.125 to 0.125
- up_weight: bfloat16 [32, 2048, 2048], P('sp', None, 'tp'), may hold values from -0.125 to 0.125
- down_weight: bfloat16 [32, 2048, 2048], P('sp', 'tp'), may hold values from -0.125 to 0.125
- out_weight: bfloat16 [2048, 2048], P(None, 'tp'), may hold values from -0.125 to 0.125
- mixer_output: bfloat16 [8192, 2048], P('sp', 'tp'), may hold values from -6 to 6
- queries: bfloat16 [8192, 2048], P('sp', 'tp'), may hold values from -6 to 6
- key_vectors: bfloat16 [8192, 2048], P('sp', 'tp'), may hold values from -0.75 to 0.75
- value_vectors: bfloat16 [8192, 2048], P('sp', 'tp'), may hold values from -6 to 6
- log_decay: float32 [8192, 32], P('sp', 'tp'), may hold values from -0.85 to 0
- block_states: bfloat16 [64, 32, 64, 64], P('sp', 'tp'), may hold values from -1.5 to 1.5
Outputs:
- grad_gate: float32 [32, 2048, 2048], P('sp', None, 'tp')
- grad_up: float32 [32, 2048, 2048], P('sp', None, 'tp')
- grad_down: float32 [32, 2048, 2048], P('sp', 'tp')
- grad_out: float32 [2048, 2048], P('sp', 'tp')
- grad_queries: bfloat16 [8192, 2048], P('sp', 'tp')
- grad_keys: bfloat16 [8192, 2048], P('sp', 'tp')
- grad_values: bfloat16 [8192, 2048], P('sp', 'tp')
Inputs may be any that keep to these rules, and one draw needn't show every extreme that they name: `routes`: each row names 2 different experts. Among the rows of one device no expert is named by more than 20 rows, and in every draw some device's rows name some expert exactly 20 times.
All inputs are finite; a program needn't handle non-finite values.
Results may differ from a plain program's by a relative error of at most 0.02.
Values may be sent and summed in bfloat16 or wider, within the bound.
A program may use at most 128 MiB of HBM per device.

v0:
```python
import jax
import jax.numpy as jnp
from jax import lax
from jax.sharding import PartitionSpec as P
from jax.experimental import pallas as pl
from jax.experimental.pallas import tpu as pltpu

EXP_DEV = 1
TOP_K = 2
SP = "sp"


clamp_limit = 7.0
sigmoid_sharpness = 1.702


MAIN = 16
LEFT = 4
LANES = 128
BF = jnp.bfloat16
F32 = jnp.float32
MESH_ID = pl.DeviceIdType.MESH


def dot(a, b):
    return jnp.dot(a, b, preferred_element_type=F32)


def dot_t(a, b):
    return lax.dot_general(a, b, (((1,), (1,)), ((), ())), preferred_element_type=F32)


def t_dot(a, b):
    return lax.dot_general(a, b, (((0,), (0,)), ((), ())), preferred_element_type=F32)


def iota(shape, dim):
    return lax.broadcasted_iota(jnp.int32, shape, dim)


def select_groups(y, rows):
    group = (iota((rows, 1), 0) % MAIN) // LEFT
    return sum(
        jnp.where(group == g, y[:, g * LANES : (g + 1) * LANES], 0.0) for g in range(MAIN // LEFT)
    )


def prep_kernel(routes, weights, x_ref, c_ref, s_in, s_gr, pm_ref, pl_ref):
    toks = x_ref.shape[0]
    rows = s_in.shape[0]
    experts = rows // MAIN
    share = x_ref.shape[1] // lax.axis_size("tp")
    cols = pl.ds(pl.multiple_of(lax.axis_index("tp") * share, share), share)
    e = iota((experts, toks), 0)
    first = routes[0:1, :] == e
    second = routes[1:2, :] == e
    chosen = first | second
    tri = (iota((toks, toks), 0) < iota((toks, toks), 1)).astype(BF)
    rank = dot(chosen.astype(F32).astype(BF), tri)
    ranks = jnp.where(chosen, rank, -1.0).astype(BF)
    owner = (iota((rows, experts), 0) // MAIN == iota((rows, experts), 1)).astype(BF)
    spread = dot(owner, ranks).astype(jnp.int32)
    place = iota((rows, toks), 0) % MAIN
    is_main = spread == place
    is_left = spread == MAIN + place % LEFT
    w = jnp.where(first, weights[0:1, :], 0.0) + jnp.where(second, weights[1:2, :], 0.0)
    w_rows = jnp.zeros((rows, toks), F32)
    for _ in range(3):
        piece = w.astype(BF)
        w_rows = w_rows + dot(owner, piece)
        w = w - piece.astype(F32)
    w_main = jnp.sum(jnp.where(is_main, w_rows, 0.0), axis=1, keepdims=True)
    w_left = jnp.sum(jnp.where(is_left, w_rows, 0.0), axis=1, keepdims=True)
    p_main = is_main.astype(F32).astype(BF)
    p_left = is_left.astype(F32).astype(BF)
    pm_ref[...] = p_main
    pl_ref[...] = p_left
    x = x_ref[:, cols]
    c = c_ref[:, cols]
    s_in[:, :share] = dot(p_main, x).astype(BF)
    s_in[:, share:] = select_groups(dot(p_left, x), rows).astype(BF)
    s_gr[:, :share] = (w_main * dot(p_main, c)).astype(BF)
    s_gr[:, share:] = (w_left * select_groups(dot(p_left, c), rows)).astype(BF)


def prep(routes, weights, x, c, experts):
    share = x.shape[1] // lax.axis_size("tp")
    rows = experts * MAIN
    sent = jax.ShapeDtypeStruct((rows, share + LANES), BF)
    table = jax.ShapeDtypeStruct((rows, x.shape[0]), BF)
    return pl.pallas_call(
        prep_kernel,
        out_shape=(sent, sent, table, table),
        in_specs=[pl.BlockSpec(memory_space=pltpu.VMEM)] * 4,
        out_specs=[pl.BlockSpec(memory_space=pltpu.VMEM)] * 4,
        compiler_params=pltpu.CompilerParams(vmem_limit_bytes=40 << 20),
        cost_estimate=pl.CostEstimate(flops=10**9, bytes_accessed=5 << 20, transcendentals=0),
        name="prep",
    )(routes, weights, x, c)


def expert_kernel(
    s_in, s_gr, wg_h, wu_h, wd_h, pm_ref, pl_ref, cot_ref,
    x_out, c_out, gg_out, ug_out, act_out, res_out,
    recv, xs, wg, wu, wd, acc, half_out, ip, far_in, near_in, ret_t, ret_q, res,
    w_sem, a_send, a_recv, g_send, g_recv, rs_send, rs_recv, t_send, t_recv, r_send, r_recv, o_sem,
):
    n_sp, n_tp = lax.axis_size("sp"), lax.axis_size("tp")
    me, tp = lax.axis_index("sp"), lax.axis_index("tp")
    nxt, prv, far = lax.rem(tp + 1, n_tp), lax.rem(tp + n_tp - 1, n_tp), lax.rem(tp + 2, n_tp)
    share = wg.shape[0] // n_tp
    wide = share + LANES
    hidden = wg.shape[1]
    hs = n_sp // 2 * MAIN
    hx = n_sp // 2 * (MAIN + LEFT)
    hl = n_sp // 2 * LEFT

    def at(k, width):
        return pl.ds(pl.multiple_of(k * width, LANES), width)

    def slab(k):
        return pl.ds(pl.multiple_of(k * MAIN, MAIN), MAIN)

    loads = [
        pltpu.make_async_copy(src, dst, w_sem.at[i])
        for i, (src, dst) in enumerate(((wg_h, wg), (wu_h, wu), (wd_h, wd)))
    ]
    for load in loads:
        load.start()

    barrier = pltpu.get_barrier_semaphore()

    def greet(i, carry):
        pl.semaphore_signal(
            barrier, inc=1, device_id={"sp": lax.rem(me + i, n_sp)}, device_id_type=MESH_ID
        )
        return carry

    lax.fori_loop(1, n_sp, greet, 0)
    for k in (nxt, prv):
        pl.semaphore_signal(barrier, inc=1, device_id={"tp": k}, device_id_type=MESH_ID)
    pl.semaphore_wait(barrier, n_sp + 1)

    for a, src in ((0, s_in), (1, s_gr)):
        landing = recv.at[a, slab(me), at(tp, wide)]
        pltpu.make_async_copy(src.at[slab(me), :], landing, a_recv.at[a, me // (n_sp // 2)]).start()

        def deliver(i, carry):
            e = lax.rem(me + i, n_sp)
            pltpu.make_async_remote_copy(
                src_ref=src.at[slab(e), :],
                dst_ref=landing,
                send_sem=a_send.at[a],
                recv_sem=a_recv.at[a, me // (n_sp // 2)],
                device_id={"sp": e},
                device_id_type=MESH_ID,
            ).start()
            return carry

        lax.fori_loop(1, n_sp, deliver, 0)

    def tp_copy(ref, dst, sends, recvs, i, k):
        return pltpu.make_async_remote_copy(
            src_ref=ref, dst_ref=dst, send_sem=sends.at[i], recv_sem=recvs.at[i],
            device_id={"tp": k}, device_id_type=MESH_ID,
        )

    def ring_copies(view, sends, recvs):
        def move(h, k, i, to):
            return tp_copy(view(h, k), view(h, k), sends, recvs, i, to)

        return [
            move(0, tp, 0, nxt), move(1, tp, 1, nxt), move(0, tp, 2, prv), move(1, tp, 3, prv),
            move(0, prv, 4, nxt), move(1, nxt, 5, prv),
        ]

    jj = iota((hs, hs), 0)
    qq = iota((hs, hs), 1)
    unpick = (
        qq == ((jj % hl) // LEFT) * MAIN + (jj // hl) * LEFT + jj % LEFT
    ).astype(F32).astype(BF)
    pick = (
        qq == ((jj % MAIN) // LEFT) * hl + (jj // MAIN) * LEFT + jj % LEFT
    ).astype(F32).astype(BF)
    groups = MAIN // LEFT

    def unpack(a, k):
        for h in range(2):
            rows = pl.ds(h * hs, hs)
            xs[a, h * hx : h * hx + hs, at(k, share)] = recv[a, rows, pl.ds(pl.multiple_of(k * wide, LANES), share)]
            tail = recv[a, rows, pl.ds(pl.multiple_of(k * wide + share, LANES), LANES)]
            spread = dot(unpick, tail).astype(BF)
            left = jnp.concatenate([spread[g * hl : (g + 1) * hl] for g in range(groups)], axis=1)
            xs[a, h * hx + hs : (h + 1) * hx, at(k, share)] = left

    def piece_in(k, fresh):
        unpack(0, k)

        @pl.loop(0, 2)
        def _(h):
            rows = pl.ds(pl.multiple_of(h * hx, MAIN), hx)
            x = xs[0, rows, at(k, share)]
            g = dot(x, wg[at(k, share), :])
            u = dot(x, wu[at(k, share), :])
            if fresh:
                acc[0, rows, :] = g
                acc[1, rows, :] = u
            else:
                acc[0, rows, :] += g
                acc[1, rows, :] += u

    def piece_gr(k, fresh):
        unpack(1, k)

        @pl.loop(0, 2)
        def _(h):
            rows = pl.ds(pl.multiple_of(h * hx, MAIN), hx)
            d = dot_t(xs[1, rows, at(k, share)], wd[:, at(k, share)])
            if fresh:
                acc[2, rows, :] = d
            else:
                acc[2, rows, :] += d

    rings = [
        ring_copies(
            lambda h, k, a=a: recv.at[a, pl.ds(h * hs, hs), at(k, wide)],
            g_send.at[a], g_recv.at[a],
        )
        for a in range(2)
    ]

    def wait_arrivals(a, h):
        ref = recv.at[a, pl.ds(h * hs, hs), at(tp, wide)]
        pltpu.make_async_copy(ref, ref, a_recv.at[a, h]).wait()

    def ring_begin(ring, ready):
        ready(0)
        ring[0].start()
        ring[2].start()
        ready(1)
        ring[3].start()
        ring[1].start()

    def ring_relay(ring):
        ring[0].wait_recv()
        ring[4].start()
        ring[3].wait_recv()
        ring[5].start()

    ring_begin(rings[0], lambda h: wait_arrivals(0, h))
    loads[0].wait()
    loads[1].wait()
    piece_in(tp, True)
    ring_relay(rings[0])
    ring_begin(rings[1], lambda h: wait_arrivals(1, h))
    rings[0][1].wait_recv()
    piece_in(prv, False)
    rings[0][2].wait_recv()
    piece_in(nxt, False)
    loads[2].wait()
    piece_gr(tp, True)
    rings[0][4].wait_recv()
    rings[0][5].wait_recv()
    piece_in(far, False)
    x_copy = pltpu.make_async_copy(xs.at[0], x_out, o_sem.at[0])
    x_copy.start()

    step = 2 * MAIN

    @pl.loop(0, 2 * hx // step)
    def _(i):
        rows = pl.ds(pl.multiple_of(i * step, step), step)
        gate, up = acc[0, rows, :], acc[1, rows, :]
        clamped = jnp.minimum(gate, clamp_limit)
        logistic = 1.0 / (1.0 + jnp.exp(-sigmoid_sharpness * clamped))
        linear = jnp.clip(up, -clamp_limit, clamp_limit) + 1.0
        swish = clamped * logistic
        half_out[2, rows, :] = (swish * linear).astype(BF)
        slope = logistic + sigmoid_sharpness * swish * (1.0 - logistic)
        acc[0, rows, :] = jnp.where(gate < clamp_limit, linear * slope, 0.0)
        acc[1, rows, :] = jnp.where(jnp.abs(up) < clamp_limit, swish, 0.0)

    act_copy = pltpu.make_async_copy(half_out.at[2], act_out, o_sem.at[1])
    act_copy.start()

    ring_relay(rings[1])
    rings[1][1].wait_recv()
    piece_gr(prv, False)
    rings[1][2].wait_recv()
    piece_gr(nxt, False)
    rings[1][4].wait_recv()
    rings[1][5].wait_recv()
    piece_gr(far, False)
    c_copy = pltpu.make_async_copy(xs.at[1], c_out, o_sem.at[2])
    c_copy.start()

    @pl.loop(0, 2 * hx // step)
    def _(i):
        rows = pl.ds(pl.multiple_of(i * step, step), step)
        act_grad = acc[2, rows, :]
        half_out[0, rows, :] = (act_grad * acc[0, rows, :]).astype(BF)
        half_out[1, rows, :] = (act_grad * acc[1, rows, :]).astype(BF)

    gg_copy = pltpu.make_async_copy(half_out.at[0], gg_out, o_sem.at[3])
    ug_copy = pltpu.make_async_copy(half_out.at[1], ug_out, o_sem.at[4])
    gg_copy.start()
    ug_copy.start()

    def part(k, slot):
        @pl.loop(0, 2)
        def _(h):
            rows = pl.ds(pl.multiple_of(h * hx, MAIN), hx)
            y = dot_t(half_out[0, rows, :], wg[at(k, share), :])
            y = y + dot_t(half_out[1, rows, :], wu[at(k, share), :])
            ip[slot, rows, :] = y.astype(BF)

    halves = [pl.ds(0, hx), pl.ds(hx, hx)]

    def rs_copy(src, dst, i, k):
        return tp_copy(src, dst, rs_send, rs_recv, i, k)

    rs = [
        rs_copy(ip.at[0, halves[0]], far_in.at[0], 0, nxt),
        rs_copy(ip.at[0, halves[1]], far_in.at[1], 1, prv),
        rs_copy(ip.at[1, halves[1]], near_in.at[0, halves[1]], 2, nxt),
        rs_copy(ip.at[2, halves[0]], near_in.at[1, halves[0]], 3, prv),
        rs_copy(ip.at[1, halves[0]], near_in.at[0, halves[0]], 4, nxt),
        rs_copy(ip.at[2, halves[1]], near_in.at[1, halves[1]], 5, prv),
    ]
    part(far, 0)
    rs[0].start()
    rs[1].start()
    part(nxt, 1)
    rs[2].start()
    part(prv, 2)
    rs[3].start()
    rs[0].wait_recv()
    ip[1, halves[0], :] = (ip[1, halves[0], :].astype(F32) + far_in[0].astype(F32)).astype(BF)
    rs[4].start()
    rs[1].wait_recv()
    ip[2, halves[1], :] = (ip[2, halves[1], :].astype(F32) + far_in[1].astype(F32)).astype(BF)
    rs[5].start()
    part(tp, 3)

    for h in range(2):
        rs[(4, 2)[h]].wait_recv()
        rs[(3, 5)[h]].wait_recv()
        total = (
            ip[3, halves[h], :].astype(F32)
            + near_in[0, halves[h], :].astype(F32)
            + near_in[1, halves[h], :].astype(F32)
        ).astype(BF)
        ret_t[h * hs : (h + 1) * hs, :share] = total[:hs]
        stacked = jnp.concatenate(
            [total[hs:, g * LANES : (g + 1) * LANES] for g in range(groups)], axis=0
        )
        ret_t[h * hs : (h + 1) * hs, share:] = dot(pick, stacked).astype(BF)

        def give_back(i, carry):
            s = h * (n_sp // 2) + lax.rem(me + i, n_sp // 2)

            @pl.when(s != me)
            def _():
                pltpu.make_async_remote_copy(
                    src_ref=ret_t.at[slab(s), :],
                    dst_ref=ret_q.at[slab(me), :],
                    send_sem=t_send.at[0],
                    recv_sem=t_recv.at[0],
                    device_id={"sp": s},
                    device_id_type=MESH_ID,
                ).start()

            return carry

        lax.fori_loop(0, n_sp // 2, give_back, 0)
    ret_q[slab(me), :] = ret_t[slab(me), :]
    others = pl.ds(0, (n_sp - 1) * MAIN)
    pltpu.make_async_copy(ret_q.at[others, :], ret_q.at[others, :], t_recv.at[0]).wait()

    p_left = pl_ref[...]
    y = t_dot(pm_ref[...], ret_q[:, :share])
    tails = ret_q[:, share:]
    group = (iota(p_left.shape, 0) % MAIN) // LEFT
    y = y + jnp.concatenate(
        [t_dot(jnp.where(group == g, p_left, jnp.zeros_like(p_left)), tails) for g in range(groups)],
        axis=1,
    )
    res[:, at(tp, share)] = (cot_ref[:, at(tp, share)].astype(F32) + y).astype(BF)
    toks = res.shape[0]
    ring = ring_copies(
        lambda h, k: res.at[pl.ds(h * (toks // 2), toks // 2), at(k, share)], r_send, r_recv
    )
    ring_begin(ring, lambda h: None)
    ring_relay(ring)
    for i in (1, 2, 4, 5):
        ring[i].wait_recv()
    res_out[...] = res[...]

    for a in range(2):
        ref = recv.at[a, others, at(tp, wide)]
        pltpu.make_async_copy(ref, ref, a_send.at[a]).wait()
        for copy in rings[a]:
            copy.wait_send()
    for copy in rs + ring:
        copy.wait_send()
    pltpu.make_async_copy(ret_q.at[others, :], ret_q.at[others, :], t_send.at[0]).wait()
    for copy in (x_copy, act_copy, c_copy, gg_copy, ug_copy):
        copy.wait()


def expert_call(s_in, s_gr, w_gate, w_up, w_down, p_main, p_left, cotangent):
    n_sp, n_tp = lax.axis_size("sp"), lax.axis_size("tp")
    width, hidden = w_gate.shape
    rows, wide = s_in.shape
    share = width // n_tp
    full = n_sp * (MAIN + LEFT)
    toks = cotangent.shape[0]
    anyspace = pl.BlockSpec(memory_space=pl.ANY)
    vmem = pl.BlockSpec(memory_space=pltpu.VMEM)
    dma = pltpu.SemaphoreType.DMA
    return pl.pallas_call(
        expert_kernel,
        out_shape=(
            jax.ShapeDtypeStruct((full, width), BF),
            jax.ShapeDtypeStruct((full, width), BF),
            jax.ShapeDtypeStruct((full, hidden), BF),
            jax.ShapeDtypeStruct((full, hidden), BF),
            jax.ShapeDtypeStruct((full, hidden), BF),
            jax.ShapeDtypeStruct((toks, width), BF),
        ),
        in_specs=[anyspace] * 5 + [vmem] * 3,
        out_specs=[anyspace] * 5 + [vmem],
        scratch_shapes=[
            pltpu.VMEM((2, rows, n_tp * wide), BF),
            pltpu.VMEM((2, full, width), BF),
            pltpu.VMEM(w_gate.shape, BF),
            pltpu.VMEM(w_up.shape, BF),
            pltpu.VMEM(w_down.shape, BF),
            pltpu.VMEM((3, full, hidden), F32),
            pltpu.VMEM((3, full, hidden), BF),
            pltpu.VMEM((4, full, share), BF),
            pltpu.VMEM((2, full // 2, share), BF),
            pltpu.VMEM((2, full, share), BF),
            pltpu.VMEM((rows, wide), BF),
            pltpu.VMEM((rows, wide), BF),
            pltpu.VMEM((toks, width), BF),
            dma((3,)), dma((2,)), dma((2, 2)), dma((2, 6)), dma((2, 6)),
            dma((6,)), dma((6,)), dma((1,)), dma((1,)), dma((6,)), dma((6,)), dma((5,)),
        ],
        compiler_params=pltpu.CompilerParams(
            collective_id=0, has_side_effects=True, vmem_limit_bytes=60 << 20
        ),
        cost_estimate=pl.CostEstimate(flops=10**10, bytes_accessed=20 << 20, transcendentals=0),
        name="experts",
    )(s_in, s_gr, w_gate, w_up, w_down, p_main, p_left, cotangent)


def nothing_yet(x, identity):
    return jax.tree.map(
        lambda part, zero: jnp.zeros_like(part) + jnp.asarray(zero, part.dtype), x, identity
    )


def entering(x, axes, combine, identity):
    before = start = nothing_yet(x, identity)
    subtotal = x
    for axis in reversed(axes):
        peers, place = (lax.axis_size(axis), lax.axis_index(axis))
        pieces = jax.tree.map(
            lambda part, kind: lax.all_gather(part.astype(kind), axis),
            subtotal,
            (jnp.bfloat16, jnp.bfloat16),
        )
        inside, subtotal = (start, start)
        for k in reversed(range(peers)):
            passed = k > place
            subtotal = combine(
                subtotal, jax.tree.map(lambda part, own: part[k].astype(own.dtype), pieces, x)
            )
            inside = jax.tree.map(lambda new, old: jnp.where(passed, new, old), subtotal, inside)
        before = combine(inside, before)
    return before


def contract_rows(left, right):
    return lax.dot_general(
        left, right, (((0,), (0,)), ((), ())), preferred_element_type=jnp.float32
    )


def combine_suffix(earlier, later):
    return (earlier[0] * later[0], later[0][:, None, None] * earlier[1] + later[1])


def retention_grads(queries, key_vectors, value_vectors, grad_mix, log_decay, block_states):
    tok_dev = queries.shape[0]
    heads_local = log_decay.shape[1]
    head_dim = queries.shape[1] // heads_local
    blocks = block_states.shape[0]
    block_rows = tok_dev // blocks
    block_shape = (blocks, block_rows, heads_local, head_dim)
    query_blocks = queries.reshape(block_shape)
    key_blocks = key_vectors.reshape(block_shape)
    value_blocks = value_vectors.reshape(block_shape)
    grad_blocks = grad_mix.reshape(block_shape)
    cumulative = jnp.cumsum(log_decay.reshape(blocks, block_rows, heads_local), axis=1)
    block_ends = cumulative[:, -1, :]
    to_end = jnp.exp(block_ends[:, None, :] - cumulative)
    from_start = jnp.exp(cumulative)
    per_attention_head = jnp.transpose(cumulative, (0, 2, 1))
    differences = per_attention_head[:, :, :, None] - per_attention_head[:, :, None, :]
    causal = (
        jnp.arange(block_rows, dtype=jnp.int32)[:, None]
        >= jnp.arange(block_rows, dtype=jnp.int32)[None, :]
    )
    decays = jnp.where(causal, jnp.exp(jnp.minimum(differences, 0.0)), 0.0)
    grad_dot = jnp.einsum(
        "nthe,nshe->nhts", grad_blocks, value_blocks, preferred_element_type=jnp.float32
    )
    weighted_grad = (grad_dot * decays).astype(jnp.bfloat16)
    score_dot = jnp.einsum(
        "nthd,nshd->nhts", query_blocks, key_blocks, preferred_element_type=jnp.float32
    )
    weighted_score = (score_dot * decays).astype(jnp.bfloat16)
    scaled_queries = (query_blocks * from_start[..., None]).astype(jnp.bfloat16)
    outer_terms = jnp.einsum(
        "nthd,nthe->nhde", scaled_queries, grad_blocks, preferred_element_type=jnp.float32
    )
    end_factor = jnp.exp(block_ends)
    local_total = jnp.zeros((heads_local, head_dim, head_dim), jnp.float32)
    for block_id in reversed(range(blocks)):
        local_total = end_factor[block_id][:, None, None] * local_total + outer_terms[block_id]
    device_factor = jnp.exp(jnp.sum(block_ends, axis=0))
    identity = (
        jnp.ones((heads_local,), jnp.float32),
        jnp.zeros((heads_local, head_dim, head_dim), jnp.float32),
    )
    suffix = entering((device_factor, local_total), ("sp",), combine_suffix, identity)
    query_intra = jnp.einsum(
        "nhts,nshd->nthd", weighted_grad, key_blocks, preferred_element_type=jnp.float32
    )
    query_carry = jnp.einsum(
        "nthe,nhde->nthd", grad_blocks, block_states, preferred_element_type=jnp.float32
    )
    grad_queries = (
        (query_intra + query_carry * from_start[..., None])
        .astype(jnp.bfloat16)
        .reshape(tok_dev, -1)
    )
    key_intra = jnp.einsum(
        "nhts,nthd->nshd", weighted_grad, query_blocks, preferred_element_type=jnp.float32
    )
    value_intra = jnp.einsum(
        "nhts,nthe->nshe", weighted_score, grad_blocks, preferred_element_type=jnp.float32
    )
    state_grad = suffix[1]
    leaving = []
    for block_id in reversed(range(blocks)):
        leaving.append(state_grad)
        state_grad = end_factor[block_id][:, None, None] * state_grad + outer_terms[block_id]
    carried = jnp.stack(leaving[::-1], axis=0).astype(jnp.bfloat16)
    key_carry = jnp.einsum(
        "nshe,nhde->nshd", value_blocks, carried, preferred_element_type=jnp.float32
    )
    value_carry = jnp.einsum(
        "nshd,nhde->nshe", key_blocks, carried, preferred_element_type=jnp.float32
    )
    grad_keys = (
        (key_intra + key_carry * to_end[..., None]).astype(jnp.bfloat16).reshape(tok_dev, -1)
    )
    grad_values = (
        (value_intra + value_carry * to_end[..., None]).astype(jnp.bfloat16).reshape(tok_dev, -1)
    )
    return (grad_queries, grad_keys, grad_values)


def shards(
    moe_input,
    cotangent,
    routes,
    route_weights,
    gate_weight,
    up_weight,
    down_weight,
    out_weight,
    mixer_output,
    queries,
    key_vectors,
    value_vectors,
    log_decay,
    block_states,
):
    experts_total = EXP_DEV * lax.axis_size("sp")
    s_in, s_gr, p_main, p_left = prep(
        routes.T, route_weights.T, moe_input, cotangent, experts_total
    )
    rows, row_grads, gate_grad, up_grad, activation, residual_grad = expert_call(
        s_in, s_gr, gate_weight[0], up_weight[0], down_weight[0], p_main, p_left, cotangent
    )
    grad_gate = contract_rows(rows, gate_grad)[None]
    grad_up = contract_rows(rows, up_grad)[None]
    grad_down = contract_rows(activation, row_grads)[None]
    grad_out = lax.psum_scatter(
        contract_rows(residual_grad, mixer_output).astype(jnp.bfloat16),
        SP,
        scatter_dimension=0,
        tiled=True,
    ).astype(jnp.float32)
    grad_mix = jnp.dot(residual_grad, out_weight, preferred_element_type=jnp.float32).astype(
        jnp.bfloat16
    )
    grad_queries, grad_keys, grad_values = retention_grads(
        queries, key_vectors, value_vectors, grad_mix, log_decay, block_states
    )
    return (grad_gate, grad_up, grad_down, grad_out, grad_queries, grad_keys, grad_values)


def solution(mesh):
    return jax.shard_map(
        shards,
        mesh=mesh,
        in_specs=(
            P(SP, None),
            P(SP, None),
            P(SP, None),
            P(SP, None),
            P(SP, None, "tp"),
            P(SP, None, "tp"),
            P(SP, "tp", None),
            P(None, "tp"),
            P(SP, "tp"),
            P(SP, "tp"),
            P(SP, "tp"),
            P(SP, "tp"),
            P(SP, "tp"),
            P(SP, "tp", None, None),
        ),
        out_specs=(
            P(SP, None, "tp"),
            P(SP, None, "tp"),
            P(SP, "tp", None),
            P(SP, "tp"),
            P(SP, "tp"),
            P(SP, "tp"),
            P(SP, "tp"),
        ),
        check_vma=False,
    )
```

profile of v0, /device:TPU:5, one launch (start us, length us, event | category | flops | bytes accessed | tf_op | source)
XLA Modules:
  0.0 275.1 jit_solution(17546806048518112733)
XLA Ops:
  7.2 1.4 copy-done.1
  8.6 1.2 copy-done.2
  9.8 0.7 copy-done.3
  10.5 0.7 copy-done.4
  11.2 1.2 prep.1
  12.4 0.8 copy-done.5
  13.2 0.8 copy-done.6
  14.0 0.7 copy-done.7
  14.7 0.7 copy-done.8
  15.4 112.5 %experts.1 = (bf16[640,2048]{1,0:T(8,128)(2,1)}, bf16[640,2048]{1,0:T(8,128)(2,1)}, bf16[640,512]{1,0:T(8,128)(2,1)}, bf16[640,512]{1,0:T(8,128)(2,1)}, bf16[640...) custom-call(bf16[512,640]{1,0:T(8,128)(2,1)} %copy-done.5, bf16[512,640]{1,0:T(8,128)(2,1)} %copy-done.6, ...), custom_call_target="tpu_custom_call" | custom-call | flops 10000000000 | bytes 20971520 | tf_op jit(solution)/shard_map/experts/pallas_call | solution.py:421
  127.9 3.3 %convolution_convert_fusion = bf16[2048,512]{1,0:T(8,128)(2,1)} fusion(bf16[256,2048]{1,0:T(8,128)(2,1)} %get-tuple-element.26, bf16[256,512]{1,0:T(8,128)(2,1)S(1)} %copy-done.16), kind=kOutput, calls=%fused_computation.3 | convolution fusion | flops 537919488 | bytes 3407872 | tf_op jit(solution)/shard_map/dot_general | solution.py:486
  131.8 0.5 slice_reduce_fusion
  132.4 0.7 subtract_exponential_fusion
  133.1 2.1 reshape.435
  135.2 1.3 copy.74
  136.5 1.4 convolution_convert_fusion.1
  138.0 1.3 reshape.432
  139.3 0.3 copy.63
  139.6 0.6 slice_bitcast_fusion
  140.2 0.3 fusion.15
  140.5 0.8 fusion.16
  141.4 2.1 reshape.434
  143.5 1.3 copy.69
  144.9 2.1 reshape.433
  146.9 2.0 copy.64
  149.0 1.5 fusion
  150.5 0.8 copy-done.12
  151.3 0.4 convolution_bitcast_fusion.8
  151.8 0.9 fusion.8
  152.7 2.0 copy.90
  154.7 2.1 reshape.429
  156.8 0.6 dynamic-slice
  158.3 64.1 %all-reduce = bf16[256]{0:T(256)(128)(2,1)S(1)} all-reduce(bf16[256]{0:T(256)(128)(2,1)S(1)} %dynamic-update-slice), channel_id=2, replica_groups=mesh['sp'=32,'tp'=4] {'sp'}, use_global_device_ids=true, to_apply=%add | all-reduce | flops 256 | bytes 1024
  222.5 0.6 convert_multiply_fusion
  223.1 0.7 slice_convert_fusion.30
  223.8 2.1 convolution_bitcast_fusion.3
  226.0 1.5 convolution_bitcast_fusion.6
  227.4 5.9 %convolution_bitcast_fusion.2 = f32[1,2048,512]{2,1,0:T(8,128)} fusion(bf16[640,2048]{1,0:T(8,128)(2,1)} %get-tuple-element.21, bf16[640,512]{1,0:T(8,128)(2,1)} %get-tuple-element.22), kind=kOutput, calls=%fused_computation.2 | convolution fusion | flops 1342177280 | bytes 7471104 | tf_op jit(solution)/shard_map/dot_general | solution.py:486
  233.4 3.9 %convolution_bitcast_fusion.1 = f32[1,2048,512]{2,1,0:T(8,128)} fusion(bf16[640,2048]{1,0:T(8,128)(2,1)S(1)} %copy-done.27, bf16[640,512]{1,0:T(8,128)(2,1)S(1)} %copy-done.28), kind=kOutput, calls=%fused_computation.1 | convolution fusion | flops 1342177280 | bytes 7471104 | tf_op jit(solution)/shard_map/dot_general | solution.py:486
  237.3 3.9 %convolution_bitcast_fusion = f32[1,512,2048]{2,1,0:T(8,128)} fusion(bf16[640,512]{1,0:T(8,128)(2,1)S(1)} %copy-done.14, bf16[640,2048]{1,0:T(8,128)(2,1)S(1)} %copy-done.10), kind=kOutput, calls=%fused_computation | convolution fusion | flops 1342177280 | bytes 7471104 | tf_op jit(solution)/shard_map/dot_general | solution.py:486
  241.2 1.5 convert_element_type.527
  242.7 17.9 %all-gather.3.cloned.1.call-done = bf16[32,8,64,64]{3,2,1,0:T(8,128)(2,1)} async-done(((bf16[1,8,64,64]{3,2,1,0:T(8,128)(2,1)}), bf16[32,8,64,64]{3,2,1,0:T(8,128)(2,1)}) %all-gather.3.cloned.1.call-update) | async-done | bytes 2097168 | tf_op jit(solution)/shard_map/all_gather | solution.py:470
  260.6 3.4 %add_convert_fusion = (bf16[1,8,64,64]{3,2,1,0:T(8,128)(2,1)S(1)}, bf16[1,8,64,64]{3,2,1,0:T(8,128)(2,1)S(1)}) fusion(f32[2,8,64,64]{3,2,1,0:T(8,128)S(1)} %fusion.15, f32[8]{0:T(128)S(1)} %copy-done.23, pred[]{:T(512)S(6)} %lt.127, pred[]{:T(512)S(6)} %lt.126, pred[]{:T(512)S(6)} %lt.125, pred[]{:T(512)S(6)} %lt.124, pred[]{:T(512)S(6)} %lt.123, ...), kind=kLoop, calls=%fused_computation.34 | loop fusion | flops 4292608 | bytes 2360384 | tf_op jit(solution)/shard_map/convert.31
  264.0 1.3 fusion.9
  265.5 0.3 copy.91
  265.9 1.0 reshape.430
  266.9 0.3 copy.92
  267.2 1.0 reshape.431
  (67 shorter events, 1.5 us)
Async XLA Ops:
  7.2 129.4 %copy-start = (bf16[2048,512]{1,0:T(8,128)(2,1)S(1)}, bf16[2048,512]{1,0:T(8,128)(2,1)}, u32[]{:S(2)}) copy-start(bf16[2048,512]{1,0:T(8,128)(2,1)} %param.21) | copy-start | bytes 6291460
  7.2 234.0 %reduce-scatter.2.cloned.1.call-start = ((), (), s32[]{:S(2)}) async-start(), calls=%async_computation.1 | async-start | bytes 2162688 | tf_op jit(solution)/shard_map/reduce_scatter | solution.py:603
  7.2 1.4 copy-start.1
  8.6 1.2 copy-start.2
  9.8 0.7 copy-start.3
  10.5 0.7 copy-start.4
  12.4 0.8 copy-start.5
  13.2 0.8 copy-start.6
  14.0 0.7 copy-start.7
  14.7 0.7 copy-start.8
  15.4 112.5 %copy-start.16 = (bf16[256,512]{1,0:T(8,128)(2,1)S(1)}, bf16[256,512]{1,0:T(8,128)(2,1)}, u32[]{:S(2)}) copy-start(bf16[256,512]{1,0:T(8,128)(2,1)} %param.22) | copy-start | bytes 786436
  127.9 3.6 %copy-start.18 = (f32[256,8]{0,1:T(8,128)S(1)}, f32[256,8]{0,1:T(8,128)}, u32[]{:S(2)}) copy-start(f32[256,8]{0,1:T(8,128)} %param.26) | copy-start | bytes 24580
  131.2 5.3 %copy-start.9 = (bf16[256,2048]{1,0:T(8,128)(2,1)S(1)}, bf16[256,2048]{1,0:T(8,128)(2,1)}, u32[]{:S(2)}) copy-start(bf16[256,2048]{1,0:T(8,128)(2,1)} %get-tuple-element.26) | copy-start | bytes 3145732
  131.3 129.3 %all-gather.3.cloned.1.call-start = ((), (), s32[]{:S(2)}) async-start(), calls=%async_computation.2 | async-start | bytes 4325376 | tf_op jit(solution)/shard_map/all_gather | solution.py:470
  138.0 3.4 %copy-start.15 = (f32[2,128,8]{2,1,0:T(8,128)S(1)}, f32[2,128,8]{2,1,0:T(8,128)}, u32[]{:S(2)}) copy-start(f32[2,128,8]{2,1,0:T(8,128)} %get-tuple-element.45) | copy-start | bytes 24580
  148.9 2.8 %copy-start.17 = (bf16[2,8,64,64]{3,2,1,0:T(8,128)(2,1)S(1)}, bf16[2,8,64,64]{3,2,1,0:T(8,128)(2,1)}, u32[]{:S(2)}) copy-start(bf16[2,8,64,64]{3,2,1,0:T(8,128)(2,1)} %param.27) | copy-start | bytes 393220
  149.0 7.8 %copy-start.26 = (u32[128]{0:T(128)S(1)}, u32[128]{0:T(128)}, u32[]{:S(2)}) copy-start(u32[128]{0:T(128)} %constant.83) | copy-start | bytes 1540
  149.0 9.1 %copy-start.25 = (f32[8]{0:T(128)S(1)}, f32[8]{0:T(128)}, u32[]{:S(2)}) copy-start(f32[8]{0:T(128)} %get-tuple-element.43) | copy-start | bytes 100
  150.5 0.8 copy-start.12
  227.4 5.9 %copy-start.27 = (bf16[640,2048]{1,0:T(8,128)(2,1)S(1)}, bf16[640,2048]{1,0:T(8,128)(2,1)}, u32[]{:S(2)}) copy-start(bf16[640,2048]{1,0:T(8,128)(2,1)} %get-tuple-element.21) | copy-start | bytes 7864324
  227.4 5.9 %copy-start.28 = (bf16[640,512]{1,0:T(8,128)(2,1)S(1)}, bf16[640,512]{1,0:T(8,128)(2,1)}, u32[]{:S(2)}) copy-start(bf16[640,512]{1,0:T(8,128)(2,1)} %get-tuple-element.23) | copy-start | bytes 1966084
  233.4 3.9 %copy-start.10 = (bf16[640,2048]{1,0:T(8,128)(2,1)S(1)}, bf16[640,2048]{1,0:T(8,128)(2,1)}, u32[]{:S(2)}) copy-start(bf16[640,2048]{1,0:T(8,128)(2,1)} %get-tuple-element.25) | copy-start | bytes 7864324
  233.4 3.9 %copy-start.14 = (bf16[640,512]{1,0:T(8,128)(2,1)S(1)}, bf16[640,512]{1,0:T(8,128)(2,1)}, u32[]{:S(2)}) copy-start(bf16[640,512]{1,0:T(8,128)(2,1)} %get-tuple-element.24) | copy-start | bytes 1966084
  237.2 23.3 %copy-start.19 = (f32[8]{0:T(128)S(1)}, f32[8]{0:T(128)}, u32[]{:S(2)}) copy-start(f32[8]{0:T(128)} %get-tuple-element.64) | copy-start | bytes 100
  237.2 23.3 %copy-start.20 = (f32[8]{0:T(128)S(1)}, f32[8]{0:T(128)}, u32[]{:S(2)}) copy-start(f32[8]{0:T(128)} %get-tuple-element.65) | copy-start | bytes 100
  237.3 23.3 %copy-start.21 = (f32[8]{0:T(128)S(1)}, f32[8]{0:T(128)}, u32[]{:S(2)}) copy-start(f32[8]{0:T(128)} %get-tuple-element.66) | copy-start | bytes 100
  237.3 23.3 %copy-start.22 = (f32[8]{0:T(128)S(1)}, f32[8]{0:T(128)}, u32[]{:S(2)}) copy-start(f32[8]{0:T(128)} %get-tuple-element.67) | copy-start | bytes 100
  237.3 23.3 %copy-start.23 = (f32[8]{0:T(128)S(1)}, f32[8]{0:T(128)}, u32[]{:S(2)}) copy-start(f32[8]{0:T(128)} %get-tuple-element.48) | copy-start | bytes 100
  237.3 23.3 %copy-start.24 = (f32[8]{0:T(128)S(1)}, f32[8]{0:T(128)}, u32[]{:S(2)}) copy-start(f32[8]{0:T(128)} %convert_multiply_fusion) | copy-start | bytes 100
  260.6 4.7 %copy-start.11 = (f32[2,128,8,64]{1,3,2,0:T(8,128)S(1)}, f32[2,128,8,64]{1,3,2,0:T(8,128)}, u32[]{:S(2)}) copy-start(f32[2,128,8,64]{1,3,2,0:T(8,128)} %convolution_bitcast_fusion.3) | copy-start | bytes 1572868
  260.6 4.7 %copy-start.13 = (bf16[2,128,8,64]{1,3,2,0:T(8,128)(2,1)S(1)}, bf16[2,128,8,64]{1,3,2,0:T(8,128)(2,1)}, u32[]{:S(2)}) copy-start(bf16[2,128,8,64]{1,3,2,0:T(8,128)(2,1)} %copy.64) | copy-start | bytes 786436
Sparse Core Ops, SparseCore 0:
  131.4 79.3 reduce-scatter.1
  213.0 47.4 all-gather.2
where the time goes:
time: 277 us; the launch traced here: 275 us
  Pallas kernels  114 us (41%)
  blocking collectives  64.1 us (23%)
  local copies, waits for them, and re-layouts  28.9 us (10%)
  matrix products  26.7 us (10%)
  waiting for transfers between devices  17.9 us (6%)
  between operations  15.1 us (5%)
  other arithmetic  8.45 us (3%)
    pallas_call x1, Pallas kernels, expert_call(): pl.pallas_call(expert_kernel, out_shape=(jax.ShapeDtypeStruct((full, widt...  112 us
    unnamed x1, blocking collectives  64.1 us
    all_gather x1, waiting for transfers between devices, entering(): lax.all_gather(part.astype(kind), axis)  17.9 us
    dot_general x4, matrix products, contract_rows(): lax.dot_general(left, right, (((0,), (0,)), ((), ())), preferred_element_...  16.9 us
    unnamed x67, local copies, waits for them, and re-layouts  15.5 us
  transfers between devices with their start and end apart: 2, of which 1 were waited for; matrix products, arithmetic and copies ran while one was open for 16% of the time, Pallas kernels for 0%

commit v1 on v0

--- a/solution.py
+++ b/solution.py
@@ -5,8 +5,6 @@
 from jax.experimental import pallas as pl
 from jax.experimental.pallas import tpu as pltpu
 
-EXP_DEV = 1
-TOP_K = 2
 SP = "sp"
 
 
@@ -100,10 +98,14 @@
 
 
 def expert_kernel(
-    s_in, s_gr, wg_h, wu_h, wd_h, pm_ref, pl_ref, cot_ref,
-    x_out, c_out, gg_out, ug_out, act_out, res_out,
+    s_in, s_gr, wg_h, wu_h, wd_h, ow_h, mix_h, q_h, k_h, v_h, pm_ref, pl_ref, cot_ref,
+    ld_ref, st_ref,
+    x_out, c_out, gg_out, ug_out, act_out, go_out, gq_out, gk_out, gv_out,
     recv, xs, wg, wu, wd, acc, half_out, ip, far_in, near_in, ret_t, ret_q, res,
     w_sem, a_send, a_recv, g_send, g_recv, rs_send, rs_recv, t_send, t_recv, r_send, r_recv, o_sem,
+    ow, mix, qkv, cum, cum_t, decay, score, logs, gm, gmb, outer, local, part, peer, got,
+    ybuf, zbuf, lt_send, lt_recv, d_send, d_recv, b_send, b_recv, sc_send, sc_recv,
+    sy_send, sy_recv, sz_send, sz_recv, cbuf,
 ):
     n_sp, n_tp = lax.axis_size("sp"), lax.axis_size("tp")
     me, tp = lax.axis_index("sp"), lax.axis_index("tp")
@@ -123,7 +125,10 @@
 
     loads = [
         pltpu.make_async_copy(src, dst, w_sem.at[i])
-        for i, (src, dst) in enumerate(((wg_h, wg), (wu_h, wu), (wd_h, wd)))
+        for i, (src, dst) in enumerate(
+            ((wg_h, wg), (wu_h, wu), (wd_h, wd), (ow_h, ow), (mix_h, mix))
+            + tuple((src, qkv.at[j]) for j, src in enumerate((q_h, k_h, v_h)))
+        )
     ]
     for load in loads:
         load.start()
@@ -158,6 +163,77 @@
             return carry
 
         lax.fori_loop(1, n_sp, deliver, 0)
+
+    toks = res.shape[0]
+    blk = toks // 2
+    pairs = share // LANES
+    core, y_at, z_at = lax.rem(me, 2), lax.rem(me // 2, 4), me // 8
+
+    def pieces(v):
+        out = []
+        for _ in range(3):
+            p = v.astype(BF)
+            out.append(p)
+            v = v - p.astype(F32)
+        return out
+
+    heads = ld_ref.shape[1]
+    lane_head = (iota((heads, share), 1) // (share // heads) == iota((heads, share), 0)).astype(
+        F32
+    ).astype(BF)
+    lower = (iota((blk, blk), 0) >= iota((blk, blk), 1)).astype(F32).astype(BF)
+    upper = (iota((blk, blk), 0) <= iota((blk, blk), 1)).astype(F32).astype(BF)
+    for b in range(2):
+        steps = pieces(ld_ref[b * blk : (b + 1) * blk, :])
+        cum_t[b * heads : (b + 1) * heads, :] = sum(t_dot(p, upper) for p in steps)
+        cum[b * blk : (b + 1) * blk, :] = sum(
+            dot(lower, dot(p, lane_head).astype(BF)) for p in steps
+        )
+    ends = [cum[(b + 1) * blk - 1 : (b + 1) * blk, :] for b in range(2)]
+
+    def by_pair(row):
+        return jnp.concatenate(
+            [row[:, p * LANES : (p + 1) * LANES] for p in range(pairs)], axis=0
+        )
+
+    both_ends = by_pair(ends[0] + ends[1])
+    logs[me] = jnp.concatenate([both_ends, jnp.zeros_like(both_ends)], axis=0)
+
+    def tell(i, carry):
+        pltpu.make_async_remote_copy(
+            src_ref=logs.at[me],
+            dst_ref=logs.at[me],
+            send_sem=lt_send.at[0],
+            recv_sem=lt_recv.at[0],
+            device_id={"sp": lax.rem(me + i, n_sp)},
+            device_id_type=MESH_ID,
+        ).start()
+        return carry
+
+    lax.fori_loop(1, n_sp, tell, 0)
+    for load in loads[4:]:
+        load.wait()
+    low_lane = iota((1, LANES), 1) < LANES // 2
+    causal = iota((blk, blk), 0) >= iota((blk, blk), 1)
+
+    def spot(i):
+        b, p = i // pairs, lax.rem(i, pairs)
+        return pl.ds(pl.multiple_of(b * blk, blk), blk), at(p, LANES), b, p
+
+    def side(v, hh):
+        return jnp.where(low_lane if hh == 0 else ~low_lane, v, jnp.zeros_like(v))
+
+    @pl.loop(0, 2 * pairs)
+    def _(i):
+        rows, cols, b, p = spot(i)
+        q, k = qkv[0, rows, cols], qkv[1, rows, cols]
+        c = cum[rows, cols]
+        for hh in range(2):
+            column = c[:, hh * (LANES // 2) : hh * (LANES // 2) + 1]
+            row = cum_t[pl.ds(b * heads + p * 2 + hh, 1), :]
+            d = jnp.where(causal, jnp.exp(jnp.minimum(column - row, 0.0)), 0.0)
+            decay[i * 2 + hh] = d
+            score[i * 2 + hh] = (dot_t(q, side(k, hh)) * d).astype(BF)
 
     def tp_copy(ref, dst, sends, recvs, i, k):
         return pltpu.make_async_remote_copy(
@@ -306,7 +382,7 @@
     gg_copy.start()
     ug_copy.start()
 
-    def part(k, slot):
+    def expert_part(k, slot):
         @pl.loop(0, 2)
         def _(h):
             rows = pl.ds(pl.multiple_of(h * hx, MAIN), hx)
@@ -327,12 +403,12 @@
         rs_copy(ip.at[1, halves[0]], near_in.at[0, halves[0]], 4, nxt),
         rs_copy(ip.at[2, halves[1]], near_in.at[1, halves[1]], 5, prv),
     ]
-    part(far, 0)
+    expert_part(far, 0)
     rs[0].start()
     rs[1].start()
-    part(nxt, 1)
+    expert_part(nxt, 1)
     rs[2].start()
-    part(prv, 2)
+    expert_part(prv, 2)
     rs[3].start()
     rs[0].wait_recv()
     ip[1, halves[0], :] = (ip[1, halves[0], :].astype(F32) + far_in[0].astype(F32)).astype(BF)
@@ -340,7 +416,7 @@
     rs[1].wait_recv()
     ip[2, halves[1], :] = (ip[2, halves[1], :].astype(F32) + far_in[1].astype(F32)).astype(BF)
     rs[5].start()
-    part(tp, 3)
+    expert_part(tp, 3)
 
     for h in range(2):
         rs[(4, 2)[h]].wait_recv()
@@ -386,15 +462,216 @@
         axis=1,
     )
     res[:, at(tp, share)] = (cot_ref[:, at(tp, share)].astype(F32) + y).astype(BF)
-    toks = res.shape[0]
     ring = ring_copies(
         lambda h, k: res.at[pl.ds(h * (toks // 2), toks // 2), at(k, share)], r_send, r_recv
     )
     ring_begin(ring, lambda h: None)
+    block = share // (2 * pairs)
+    plane = pairs * block
+    partner = me + 1 - 2 * core
+
+    def sp_copy(src, dst, send_sem, recv_sem, e):
+        return pltpu.make_async_remote_copy(
+            src_ref=src, dst_ref=dst, send_sem=send_sem, recv_sem=recv_sem,
+            device_id={"sp": e}, device_id_type=MESH_ID,
+        )
+
+    order = (tp, prv, nxt, far)
+
+    def plane_rows(k):
+        return pl.ds(pl.multiple_of(k * plane, plane), plane)
+
+    swaps = [
+        sp_copy(
+            part.at[1 - core, plane_rows(k), :], peer.at[plane_rows(k), :],
+            d_send.at[i], d_recv.at[i], partner,
+        )
+        for i, k in enumerate(order)
+    ]
+
+    def piece_res(i):
+        k = order[i]
+        r = res[:, at(k, share)]
+        y = dot(r, ow[at(k, share), :])
+        if i == 0:
+            gm[...] = y
+        else:
+            gm[...] += y
+        for j in range(pairs):
+            g = t_dot(r[:, j * LANES : (j + 1) * LANES], mix[...]).astype(BF)
+            for c in range(2):
+                part[c, pl.ds(pl.multiple_of(k * plane + j * block, block), block), :] = g[
+                    c * block : (c + 1) * block
+                ]
+        swaps[i].start()
+
+    loads[3].wait()
+    piece_res(0)
     ring_relay(ring)
-    for i in (1, 2, 4, 5):
-        ring[i].wait_recv()
-    res_out[...] = res[...]
+    ring[1].wait_recv()
+    piece_res(1)
+    ring[2].wait_recv()
+    piece_res(2)
+    ring[4].wait_recv()
+    ring[5].wait_recv()
+    piece_res(3)
+    gmb[...] = gm[...].astype(BF)
+
+    half = LANES // 2
+
+    @pl.loop(0, 2 * pairs)
+    def _(i):
+        rows, cols, b, p = spot(i)
+        q = (qkv[0, rows, cols].astype(F32) * jnp.exp(cum[rows, cols])).astype(BF)
+        o = t_dot(q, gmb[rows, cols])
+        outer[b, p] = jnp.where(low_lane, o[:half], o[half:])
+
+    def pair_rows(tile):
+        return tile[:pairs][:, None, :]
+
+    block_factor = [jnp.exp(by_pair(e))[:, None, :] for e in ends]
+    total = block_factor[0] * outer[1] + outer[0]
+    local[0] = total.astype(BF)
+    swap_state = sp_copy(local.at[0], cbuf, sc_send.at[0], sc_recv.at[0], partner)
+    swap_state.start()
+    tiles = pl.ds(0, n_sp - 1)
+    pltpu.make_async_copy(logs.at[tiles], logs.at[tiles], lt_recv.at[0]).wait()
+
+    def chip_log(z, y):
+        return logs[z * 8 + y * 2] + logs[z * 8 + y * 2 + 1]
+
+    later_core_log = logs[me - core + 1]
+    earlier_core_log = logs[me - core]
+
+    swap_state.wait_recv()
+    mine, others_total = local[0].astype(F32), cbuf[...].astype(F32)
+    early = jnp.where(core == 0, mine, others_total)
+    late = jnp.where(core == 0, others_total, mine)
+    chip_total = jnp.exp(pair_rows(earlier_core_log)) * late + early
+    ybuf[y_at] = chip_total.astype(BF)
+    y_sends = [
+        sp_copy(
+            ybuf.at[y_at], ybuf.at[y_at], sy_send.at[i - 1], sy_recv.at[i - 1],
+            z_at * 8 + lax.rem(y_at + i, 4) * 2 + core,
+        )
+        for i in range(1, 4)
+    ]
+    for copy in y_sends:
+        copy.start()
+
+    my_block = me // 2
+
+    def send_plane(i):
+        k = order[i]
+        swaps[i].wait_recv()
+        rows = plane_rows(k)
+        part[core, rows, :] = (
+            part[core, rows, :].astype(F32) + peer[rows, :].astype(F32)
+        ).astype(BF)
+        for j in range(4):
+            zy = k * 4 + lax.rem(y_at + j, 4)
+
+            @pl.when(zy != my_block)
+            def _():
+                sp_copy(
+                    part.at[core, pl.ds(pl.multiple_of(zy * block, block), block), :],
+                    got.at[my_block], b_send.at[0], b_recv.at[0], zy * 2 + core,
+                ).start()
+
+    send_plane(0)
+    send_plane(1)
+    for copy in y_sends:
+        copy.wait_recv()
+    inside_y = jnp.zeros_like(total)
+    plane_total = jnp.zeros_like(total)
+    later_y = jnp.zeros((2 * pairs, LANES), F32)
+    for y in (3, 2, 1, 0):
+        log = chip_log(z_at, y)
+        factor = jnp.exp(pair_rows(log))
+        t = ybuf[y].astype(F32)
+        inside_y = jnp.where(y > y_at, factor * inside_y + t, inside_y)
+        later_y = jnp.where(y > y_at, later_y + log, later_y)
+        plane_total = factor * plane_total + t
+    local[1] = plane_total.astype(BF)
+    z_sends = [
+        sp_copy(local.at[1], zbuf.at[i - 1], sz_send.at[i - 1], sz_recv.at[i - 1], me - i * 8)
+        for i in range(1, 4)
+    ]
+    for i, copy in enumerate(z_sends, 1):
+
+        @pl.when(z_at >= i)
+        def _():
+            copy.start()
+
+    send_plane(2)
+    send_plane(3)
+
+    @pl.loop(0, 2 * pairs)
+    def _(i):
+        rows, cols, b, p = spot(i)
+        q, k, v, g = qkv[0, rows, cols], qkv[1, rows, cols], qkv[2, rows, cols], gmb[rows, cols]
+        outs = []
+        for hh in range(2):
+            wg_ts = (dot_t(g, side(v, hh)) * decay[i * 2 + hh]).astype(BF)
+            outs.append((dot(wg_ts, k), t_dot(wg_ts, q), t_dot(score[i * 2 + hh], g)))
+        intra = [jnp.where(low_lane, lo, hi) for lo, hi in zip(*outs)]
+        st = st_ref[b, p]
+        full = jnp.concatenate([side(st, 0), side(st, 1)], axis=0)
+        carry = dot_t(g, full) * jnp.exp(cum[rows, cols])
+        gq_out[rows, cols] = (intra[0] + carry).astype(BF)
+        gm[rows, cols] = intra[1]
+        acc[0, rows, cols] = intra[2]
+
+    beyond = jnp.zeros_like(total)
+    local_state = acc.at[1, pl.ds(0, pairs * half), pl.ds(0, LANES)]
+    local_state[...] = jnp.zeros((pairs * half, LANES), F32)
+    for i in (3, 2, 1):
+
+        @pl.when(z_at + i < 4)
+        def _():
+            z_sends[i - 1].wait_recv()
+            log = sum(chip_log(z_at + i, y) for y in range(4))
+            now = local_state[...].reshape(pairs, half, LANES)
+            now = jnp.exp(pair_rows(log)) * now + zbuf[i - 1].astype(F32)
+            local_state[...] = now.reshape(pairs * half, LANES)
+
+    beyond = local_state[...].reshape(pairs, half, LANES)
+    entering_state = jnp.exp(pair_rows(later_y)) * beyond + inside_y
+    entering_state = jnp.where(
+        core == 0, jnp.exp(pair_rows(later_core_log)) * entering_state + late, entering_state
+    )
+    carried = (block_factor[1] * entering_state + outer[1], entering_state)
+    for b in range(2):
+        outer[b] = carried[b]
+
+    @pl.loop(0, 2 * pairs)
+    def _(i):
+        rows, cols, b, p = spot(i)
+        k, v = qkv[1, rows, cols], qkv[2, rows, cols]
+        st = outer[b, p].astype(BF)
+        full = jnp.concatenate([side(st, 0), side(st, 1)], axis=0)
+        c = cum[rows, cols]
+        to_end = jnp.exp(c[blk - 1 : blk, :] - c)
+        gk_out[rows, cols] = (gm[rows, cols] + dot_t(v, full) * to_end).astype(BF)
+        gv_out[rows, cols] = (acc[0, rows, cols] + dot(k, full) * to_end).astype(BF)
+
+    blocks = pl.ds(0, 15)
+    pltpu.make_async_copy(got.at[blocks], got.at[blocks], b_recv.at[0]).wait()
+    got[my_block] = part[core, pl.ds(pl.multiple_of(my_block * block, block), block), :]
+    sums = got[0].astype(F32)
+    for i in range(1, 16):
+        sums = sums + got[i].astype(F32)
+    go_out[...] = sums
+
+    pltpu.make_async_copy(got.at[blocks], got.at[blocks], b_send.at[0]).wait()
+    pltpu.make_async_copy(logs.at[tiles], logs.at[tiles], lt_send.at[0]).wait()
+    for copy in swaps + [swap_state] + y_sends:
+        copy.wait_send()
+    for i, copy in enumerate(z_sends, 1):
+
+        @pl.when(z_at >= i)
+        def _():
+            copy.wait_send()
 
     for a in range(2):
         ref = recv.at[a, others, at(tp, wide)]
@@ -408,7 +685,10 @@
         copy.wait()
 
 
-def expert_call(s_in, s_gr, w_gate, w_up, w_down, p_main, p_left, cotangent):
+def expert_call(
+    s_in, s_gr, w_gate, w_up, w_down, w_out, mixer, queries, key_vectors, value_vectors,
+    p_main, p_left, cotangent, log_decay, states,
+):
     n_sp, n_tp = lax.axis_size("sp"), lax.axis_size("tp")
     width, hidden = w_gate.shape
     rows, wide = s_in.shape
@@ -426,10 +706,13 @@
             jax.ShapeDtypeStruct((full, hidden), BF),
             jax.ShapeDtypeStruct((full, hidden), BF),
             jax.ShapeDtypeStruct((full, hidden), BF),
-            jax.ShapeDtypeStruct((toks, width), BF),
+            jax.ShapeDtypeStruct((width // n_sp, share), F32),
+            jax.ShapeDtypeStruct((toks, share), BF),
+            jax.ShapeDtypeStruct((toks, share), BF),
+            jax.ShapeDtypeStruct((toks, share), BF),
         ),
-        in_specs=[anyspace] * 5 + [vmem] * 3,
-        out_specs=[anyspace] * 5 + [vmem],
+        in_specs=[anyspace] * 10 + [vmem] * 5,
+        out_specs=[anyspace] * 5 + [vmem] * 4,
         scratch_shapes=[
             pltpu.VMEM((2, rows, n_tp * wide), BF),
             pltpu.VMEM((2, full, width), BF),
@@ -444,134 +727,44 @@
             pltpu.VMEM((rows, wide), BF),
             pltpu.VMEM((rows, wide), BF),
             pltpu.VMEM((toks, width), BF),
-            dma((3,)), dma((2,)), dma((2, 2)), dma((2, 6)), dma((2, 6)),
+            dma((8,)), dma((2,)), dma((2, 2)), dma((2, 6)), dma((2, 6)),
             dma((6,)), dma((6,)), dma((1,)), dma((1,)), dma((6,)), dma((6,)), dma((5,)),
+            pltpu.VMEM(w_out.shape, BF),
+            pltpu.VMEM(mixer.shape, BF),
+            pltpu.VMEM((3, toks, share), BF),
+            pltpu.VMEM((toks, share), F32),
+            pltpu.VMEM((2 * log_decay.shape[1], toks // 2), F32),
+            pltpu.VMEM((16, toks // 2, toks // 2), F32),
+            pltpu.VMEM((16, toks // 2, toks // 2), BF),
+            pltpu.VMEM((n_sp, 8, LANES), F32),
+            pltpu.VMEM((toks, share), F32),
+            pltpu.VMEM((toks, share), BF),
+            pltpu.VMEM((2, 4, 64, LANES), F32),
+            pltpu.VMEM((2, 4, 64, LANES), BF),
+            pltpu.VMEM((2, width // 2, share), BF),
+            pltpu.VMEM((width // 2, share), BF),
+            pltpu.VMEM((16, width // n_sp, share), BF),
+            pltpu.VMEM((4, 4, 64, LANES), BF),
+            pltpu.VMEM((3, 4, 64, LANES), BF),
+            dma((1,)), dma((1,)), dma((4,)), dma((4,)), dma((1,)), dma((1,)), dma((1,)),
+            dma((1,)), dma((3,)), dma((3,)), dma((3,)), dma((3,)),
+            pltpu.VMEM((4, 64, LANES), BF),
         ],
         compiler_params=pltpu.CompilerParams(
             collective_id=0, has_side_effects=True, vmem_limit_bytes=60 << 20
         ),
         cost_estimate=pl.CostEstimate(flops=10**10, bytes_accessed=20 << 20, transcendentals=0),
         name="experts",
-    )(s_in, s_gr, w_gate, w_up, w_down, p_main, p_left, cotangent)
-
-
-def nothing_yet(x, identity):
-    return jax.tree.map(
-        lambda part, zero: jnp.zeros_like(part) + jnp.asarray(zero, part.dtype), x, identity
+    )(
+        s_in, s_gr, w_gate, w_up, w_down, w_out, mixer, queries, key_vectors, value_vectors,
+        p_main, p_left, cotangent, log_decay, states,
     )
-
-
-def entering(x, axes, combine, identity):
-    before = start = nothing_yet(x, identity)
-    subtotal = x
-    for axis in reversed(axes):
-        peers, place = (lax.axis_size(axis), lax.axis_index(axis))
-        pieces = jax.tree.map(
-            lambda part, kind: lax.all_gather(part.astype(kind), axis),
-            subtotal,
-            (jnp.bfloat16, jnp.bfloat16),
-        )
-        inside, subtotal = (start, start)
-        for k in reversed(range(peers)):
-            passed = k > place
-            subtotal = combine(
-                subtotal, jax.tree.map(lambda part, own: part[k].astype(own.dtype), pieces, x)
-            )
-            inside = jax.tree.map(lambda new, old: jnp.where(passed, new, old), subtotal, inside)
-        before = combine(inside, before)
-    return before
 
 
 def contract_rows(left, right):
     return lax.dot_general(
         left, right, (((0,), (0,)), ((), ())), preferred_element_type=jnp.float32
     )
-
-
-def combine_suffix(earlier, later):
-    return (earlier[0] * later[0], later[0][:, None, None] * earlier[1] + later[1])
-
-
-def retention_grads(queries, key_vectors, value_vectors, grad_mix, log_decay, block_states):
-    tok_dev = queries.shape[0]
-    heads_local = log_decay.shape[1]
-    head_dim = queries.shape[1] // heads_local
-    blocks = block_states.shape[0]
-    block_rows = tok_dev // blocks
-    block_shape = (blocks, block_rows, heads_local, head_dim)
-    query_blocks = queries.reshape(block_shape)
-    key_blocks = key_vectors.reshape(block_shape)
-    value_blocks = value_vectors.reshape(block_shape)
-    grad_blocks = grad_mix.reshape(block_shape)
-    cumulative = jnp.cumsum(log_decay.reshape(blocks, block_rows, heads_local), axis=1)
-    block_ends = cumulative[:, -1, :]
-    to_end = jnp.exp(block_ends[:, None, :] - cumulative)
-    from_start = jnp.exp(cumulative)
-    per_attention_head = jnp.transpose(cumulative, (0, 2, 1))
-    differences = per_attention_head[:, :, :, None] - per_attention_head[:, :, None, :]
-    causal = (
-        jnp.arange(block_rows, dtype=jnp.int32)[:, None]
-        >= jnp.arange(block_rows, dtype=jnp.int32)[None, :]
-    )
-    decays = jnp.where(causal, jnp.exp(jnp.minimum(differences, 0.0)), 0.0)
-    grad_dot = jnp.einsum(
-        "nthe,nshe->nhts", grad_blocks, value_blocks, preferred_element_type=jnp.float32
-    )
-    weighted_grad = (grad_dot * decays).astype(jnp.bfloat16)
-    score_dot = jnp.einsum(
-        "nthd,nshd->nhts", query_blocks, key_blocks, preferred_element_type=jnp.float32
-    )
-    weighted_score = (score_dot * decays).astype(jnp.bfloat16)
-    scaled_queries = (query_blocks * from_start[..., None]).astype(jnp.bfloat16)
-    outer_terms = jnp.einsum(
-        "nthd,nthe->nhde", scaled_queries, grad_blocks, preferred_element_type=jnp.float32
-    )
-    end_factor = jnp.exp(block_ends)
-    local_total = jnp.zeros((heads_local, head_dim, head_dim), jnp.float32)
-    for block_id in reversed(range(blocks)):
-        local_total = end_factor[block_id][:, None, None] * local_total + outer_terms[block_id]
-    device_factor = jnp.exp(jnp.sum(block_ends, axis=0))
-    identity = (
-        jnp.ones((heads_local,), jnp.float32),
-        jnp.zeros((heads_local, head_dim, head_dim), jnp.float32),
-    )
-    suffix = entering((device_factor, local_total), ("sp",), combine_suffix, identity)
-    query_intra = jnp.einsum(
-        "nhts,nshd->nthd", weighted_grad, key_blocks, preferred_element_type=jnp.float32
-    )
-    query_carry = jnp.einsum(
-        "nthe,nhde->nthd", grad_blocks, block_states, preferred_element_type=jnp.float32
-    )
-    grad_queries = (
-        (query_intra + query_carry * from_start[..., None])
-        .astype(jnp.bfloat16)
-        .reshape(tok_dev, -1)
-    )
-    key_intra = jnp.einsum(
-        "nhts,nthd->nshd", weighted_grad, query_blocks, preferred_element_type=jnp.float32
-    )
-    value_intra = jnp.einsum(
-        "nhts,nthe->nshe", weighted_score, grad_blocks, preferred_element_type=jnp.float32
-    )
-    state_grad = suffix[1]
-    leaving = []
-    for block_id in reversed(range(blocks)):
-        leaving.append(state_grad)
-        state_grad = end_factor[block_id][:, None, None] * state_grad + outer_terms[block_id]
-    carried = jnp.stack(leaving[::-1], axis=0).astype(jnp.bfloat16)
-    key_carry = jnp.einsum(
-        "nshe,nhde->nshd", value_blocks, carried, preferred_element_type=jnp.float32
-    )
-    value_carry = jnp.einsum(
-        "nshd,nhde->nshe", key_blocks, carried, preferred_element_type=jnp.float32
-    )
-    grad_keys = (
-        (key_intra + key_carry * to_end[..., None]).astype(jnp.bfloat16).reshape(tok_dev, -1)
-    )
-    grad_values = (
-        (value_intra + value_carry * to_end[..., None]).astype(jnp.bfloat16).reshape(tok_dev, -1)
-    )
-    return (grad_queries, grad_keys, grad_values)
 
 
 def shards(
@@ -590,28 +783,21 @@
     log_decay,
     block_states,
 ):
-    experts_total = EXP_DEV * lax.axis_size("sp")
     s_in, s_gr, p_main, p_left = prep(
-        routes.T, route_weights.T, moe_input, cotangent, experts_total
+        routes.T, route_weights.T, moe_input, cotangent, lax.axis_size("sp")
     )
-    rows, row_grads, gate_grad, up_grad, activation, residual_grad = expert_call(
-        s_in, s_gr, gate_weight[0], up_weight[0], down_weight[0], p_main, p_left, cotangent
+    blocks, heads, dim, _ = block_states.shape
+    states = block_states.reshape(blocks, heads // 2, 2, dim, dim)
+    states = jnp.swapaxes(states, 2, 3).reshape(blocks, heads // 2, dim, 2 * dim)
+    rows, row_grads, gate_grad, up_grad, activation, grad_out, grad_queries, grad_keys, grad_values = (
+        expert_call(
+            s_in, s_gr, gate_weight[0], up_weight[0], down_weight[0], out_weight, mixer_output,
+            queries, key_vectors, value_vectors, p_main, p_left, cotangent, log_decay, states,
+        )
     )
     grad_gate = contract_rows(rows, gate_grad)[None]
     grad_up = contract_rows(rows, up_grad)[None]
     grad_down = contract_rows(activation, row_grads)[None]
-    grad_out = lax.psum_scatter(
-        contract_rows(residual_grad, mixer_output).astype(jnp.bfloat16),
-        SP,
-        scatter_dimension=0,
-        tiled=True,
-    ).astype(jnp.float32)
-    grad_mix = jnp.dot(residual_grad, out_weight, preferred_element_type=jnp.float32).astype(
-        jnp.bfloat16
-    )
-    grad_queries, grad_keys, grad_values = retention_grads(
-        queries, key_vectors, value_vectors, grad_mix, log_decay, block_states
-    )
     return (grad_gate, grad_up, grad_down, grad_out, grad_queries, grad_keys, grad_values)
 
 

time: 277 us -> 171 us (0.62)
  blocking collectives: 64.1 us -> 0 us
  Pallas kernels: 114 us -> 143 us
  waiting for transfers between devices: 17.9 us -> 0 us
  local copies, waits for them, and re-layouts: 28.9 us -> 13.2 us
  between operations: 15.1 us -> 0.72 us
  matrix products: 26.7 us -> 13.6 us
  other arithmetic: 8.45 us -> 0 us
    unnamed x1 -> x0, blocking collectives: 64.1 us -> none
    pallas_call x1, Pallas kernels: 112 us -> 142 us  [expert_call(): pl.pallas_call(expert_kernel, out_shape=(jax.ShapeDtypeStruct((full, widt...]
    all_gather x1 -> x0, waiting for transfers between devices: 17.9 us -> none  [entering(): lax.all_gather(part.astype(kind), axis)]
    reshape x9 -> x2, local copies, waits for them, and re-layouts: 12.7 us -> 2.03 us  [the longest x1 1.22 us: shards(): states = block_states.reshape(blocks, heads // 2, 2, dim, dim)]
    dot_general x9 -> x0, matrix products: 9.76 us -> none  [the longest x1 2.14 us: retention_grads(): jnp.einsum('nhts,nthd->nshd', weighted_grad, query_blocks, preferred_elem...]
    unnamed x67 -> x37, local copies, waits for them, and re-layouts: 15.5 us -> 11.2 us
    another operation x2 -> x0, other arithmetic: 3.57 us -> none
    dot_general x4 -> x3, matrix products: 16.9 us -> 13.6 us  [contract_rows(): lax.dot_general(left, right, (((0,), (0,)), ((), ())), preferred_element_...]
  transfers between devices with their start and end apart: 2 -> 0, of which waited for: 1 -> 0; matrix products, arithmetic and copies ran while one was open for 16% -> 0% of each run, Pallas kernels for 0% -> 0%
where the time goes in v1:
time: 171 us
  Pallas kernels  143 us (84%)
  matrix products  13.6 us (8%)
  local copies, waits for them, and re-layouts  13.2 us (8%)
    pallas_call x1, Pallas kernels, expert_call(): pl.pallas_call(expert_kernel, out_shape=(jax.ShapeDtypeStruct((full, widt...  142 us
    dot_general x3, matrix products, contract_rows(): lax.dot_general(left, right, (((0,), (0,)), ((), ())), preferred_element_...  13.6 us
    unnamed x37, local copies, waits for them, and re-layouts  11.2 us

profile of v1, /device:TPU:5, one launch (start us, length us, event | category | flops | bytes accessed | tf_op | source)
XLA Modules:
  0.0 170.9 jit_solution(17072383881628311782)
XLA Ops:
  0.6 1.5 copy.22.ld_ref
  2.1 1.2 copy.24
  3.3 0.8 reshape.21.st_ref
  4.2 0.0 copy-start
  4.2 1.2 copy-done
  5.4 0.0 copy-start.1
  5.4 1.2 copy-done.1
  6.6 0.0 copy-start.2
  6.6 0.7 copy-done.2
  7.3 0.0 copy-start.3
  7.3 0.7 copy-done.3
  8.0 1.2 prep.1
  9.1 0.0 copy-start.4
  9.1 0.8 copy-done.4
  10.0 0.0 copy-start.5
  10.0 0.8 copy-done.5
  10.8 0.0 copy-start.6
  10.8 0.7 copy-done.6
  11.5 0.0 copy-start.7
  11.5 0.7 copy-done.7
  12.2 142.2 %experts.1 = (bf16[640,2048]{1,0:T(8,128)(2,1)}, bf16[640,2048]{1,0:T(8,128)(2,1)}, bf16[640,512]{1,0:T(8,128)(2,1)}, bf16[640,512]{1,0:T(8,128)(2,1)}, bf16[640...) custom-call(bf16[512,640]{1,0:T(8,128)(2,1)} %copy-done.4, ...), custom_call_target="tpu_custom_call" | custom-call | flops 10000000000 | bytes 20971520 | tf_op jit(solution)/shard_map/experts/pallas_call | solution.py:701
  154.4 0.0 copy-start.14
  154.4 0.0 copy-start.15
  154.5 5.9 %convolution_bitcast_fusion.2 = f32[1,2048,512]{2,1,0:T(8,128)} fusion(bf16[640,2048]{1,0:T(8,128)(2,1)} %get-tuple-element.24, bf16[640,512]{1,0:T(8,128)(2,1)} %get-tuple-element.25), kind=kOutput, calls=%fused_computation.2 | convolution fusion | flops 1342177280 | bytes 7471104 | tf_op jit(solution)/shard_map/dot_general | solution.py:765
  160.3 0.0 copy-done.14
  160.3 0.0 copy-done.15
  160.3 0.0 copy-start.8
  160.3 0.0 copy-start.9
  160.3 3.9 %convolution_bitcast_fusion.1 = f32[1,2048,512]{2,1,0:T(8,128)} fusion(bf16[640,2048]{1,0:T(8,128)(2,1)S(1)} %copy-done.14, bf16[640,512]{1,0:T(8,128)(2,1)S(1)} %copy-done.15), kind=kOutput, calls=%fused_computation.1 | convolution fusion | flops 1342177280 | bytes 7471104 | tf_op jit(solution)/shard_map/dot_general | solution.py:765
  164.2 0.0 copy-done.8
  164.2 0.0 copy-done.9
  164.2 0.0 copy-start.13
  164.2 0.0 copy-start.12
  164.2 0.0 copy-start.11
  164.2 0.0 copy-start.10
  164.2 3.9 %convolution_bitcast_fusion = f32[1,512,2048]{2,1,0:T(8,128)} fusion(bf16[640,512]{1,0:T(8,128)(2,1)S(1)} %copy-done.9, bf16[640,2048]{1,0:T(8,128)(2,1)S(1)} %copy-done.8), kind=kOutput, calls=%fused_computation | convolution fusion | flops 1342177280 | bytes 7471104 | tf_op jit(solution)/shard_map/dot_general | solution.py:765
  168.1 0.0 copy-done.13
  168.1 0.7 copy.29
  168.8 0.0 copy-done.12
  168.8 0.7 copy.30
  169.5 0.0 copy-done.11
  169.5 0.7 copy.31
  170.2 0.0 copy-done.10
  170.2 0.7 copy.32
Async XLA Ops:
  4.2 1.2 copy-start
  5.4 1.2 copy-start.1
  6.6 0.7 copy-start.2
  7.3 0.7 copy-start.3
  9.1 0.8 copy-start.4
  10.0 0.8 copy-start.5
  10.8 0.7 copy-start.6
  11.5 0.7 copy-start.7
  154.4 5.9 %copy-start.14 = (bf16[640,2048]{1,0:T(8,128)(2,1)S(1)}, bf16[640,2048]{1,0:T(8,128)(2,1)}, u32[]{:S(2)}) copy-start(bf16[640,2048]{1,0:T(8,128)(2,1)} %get-tuple-element.24) | copy-start | bytes 7864324
  154.4 5.9 %copy-start.15 = (bf16[640,512]{1,0:T(8,128)(2,1)S(1)}, bf16[640,512]{1,0:T(8,128)(2,1)}, u32[]{:S(2)}) copy-start(bf16[640,512]{1,0:T(8,128)(2,1)} %get-tuple-element.26) | copy-start | bytes 1966084
  160.3 3.9 %copy-start.8 = (bf16[640,2048]{1,0:T(8,128)(2,1)S(1)}, bf16[640,2048]{1,0:T(8,128)(2,1)}, u32[]{:S(2)}) copy-start(bf16[640,2048]{1,0:T(8,128)(2,1)} %get-tuple-element.28) | copy-start | bytes 7864324
  160.3 3.9 %copy-start.9 = (bf16[640,512]{1,0:T(8,128)(2,1)S(1)}, bf16[640,512]{1,0:T(8,128)(2,1)}, u32[]{:S(2)}) copy-start(bf16[640,512]{1,0:T(8,128)(2,1)} %get-tuple-element.27) | copy-start | bytes 1966084
  164.2 3.9 %copy-start.13 = (f32[64,512]{1,0:T(8,128)S(1)}, f32[64,512]{1,0:T(8,128)}, u32[]{:S(2)}) copy-start(f32[64,512]{1,0:T(8,128)} %get-tuple-element.43) | copy-start | bytes 393220
  164.2 4.5 %copy-start.12 = (bf16[256,512]{1,0:T(8,128)(2,1)S(1)}, bf16[256,512]{1,0:T(8,128)(2,1)}, u32[]{:S(2)}) copy-start(bf16[256,512]{1,0:T(8,128)(2,1)} %get-tuple-element.44) | copy-start | bytes 786436
  164.2 5.2 %copy-start.11 = (bf16[256,512]{1,0:T(8,128)(2,1)S(1)}, bf16[256,512]{1,0:T(8,128)(2,1)}, u32[]{:S(2)}) copy-start(bf16[256,512]{1,0:T(8,128)(2,1)} %get-tuple-element.45) | copy-start | bytes 786436
  164.2 5.9 %copy-start.10 = (bf16[256,512]{1,0:T(8,128)(2,1)S(1)}, bf16[256,512]{1,0:T(8,128)(2,1)}, u32[]{:S(2)}) copy-start(bf16[256,512]{1,0:T(8,128)(2,1)} %get-tuple-element.46) | copy-start | bytes 786436

commit v2 on v1

--- a/solution.py
+++ b/solution.py
@@ -6,6 +6,7 @@
 from jax.experimental.pallas import tpu as pltpu
 
 SP = "sp"
+WEIGHT_STEPS = 8
 
 
 clamp_limit = 7.0
@@ -36,76 +37,16 @@
     return lax.broadcasted_iota(jnp.int32, shape, dim)
 
 
-def select_groups(y, rows):
-    group = (iota((rows, 1), 0) % MAIN) // LEFT
-    return sum(
-        jnp.where(group == g, y[:, g * LANES : (g + 1) * LANES], 0.0) for g in range(MAIN // LEFT)
-    )
-
-
-def prep_kernel(routes, weights, x_ref, c_ref, s_in, s_gr, pm_ref, pl_ref):
-    toks = x_ref.shape[0]
-    rows = s_in.shape[0]
-    experts = rows // MAIN
-    share = x_ref.shape[1] // lax.axis_size("tp")
-    cols = pl.ds(pl.multiple_of(lax.axis_index("tp") * share, share), share)
-    e = iota((experts, toks), 0)
-    first = routes[0:1, :] == e
-    second = routes[1:2, :] == e
-    chosen = first | second
-    tri = (iota((toks, toks), 0) < iota((toks, toks), 1)).astype(BF)
-    rank = dot(chosen.astype(F32).astype(BF), tri)
-    ranks = jnp.where(chosen, rank, -1.0).astype(BF)
-    owner = (iota((rows, experts), 0) // MAIN == iota((rows, experts), 1)).astype(BF)
-    spread = dot(owner, ranks).astype(jnp.int32)
-    place = iota((rows, toks), 0) % MAIN
-    is_main = spread == place
-    is_left = spread == MAIN + place % LEFT
-    w = jnp.where(first, weights[0:1, :], 0.0) + jnp.where(second, weights[1:2, :], 0.0)
-    w_rows = jnp.zeros((rows, toks), F32)
-    for _ in range(3):
-        piece = w.astype(BF)
-        w_rows = w_rows + dot(owner, piece)
-        w = w - piece.astype(F32)
-    w_main = jnp.sum(jnp.where(is_main, w_rows, 0.0), axis=1, keepdims=True)
-    w_left = jnp.sum(jnp.where(is_left, w_rows, 0.0), axis=1, keepdims=True)
-    p_main = is_main.astype(F32).astype(BF)
-    p_left = is_left.astype(F32).astype(BF)
-    pm_ref[...] = p_main
-    pl_ref[...] = p_left
-    x = x_ref[:, cols]
-    c = c_ref[:, cols]
-    s_in[:, :share] = dot(p_main, x).astype(BF)
-    s_in[:, share:] = select_groups(dot(p_left, x), rows).astype(BF)
-    s_gr[:, :share] = (w_main * dot(p_main, c)).astype(BF)
-    s_gr[:, share:] = (w_left * select_groups(dot(p_left, c), rows)).astype(BF)
-
-
-def prep(routes, weights, x, c, experts):
-    share = x.shape[1] // lax.axis_size("tp")
-    rows = experts * MAIN
-    sent = jax.ShapeDtypeStruct((rows, share + LANES), BF)
-    table = jax.ShapeDtypeStruct((rows, x.shape[0]), BF)
-    return pl.pallas_call(
-        prep_kernel,
-        out_shape=(sent, sent, table, table),
-        in_specs=[pl.BlockSpec(memory_space=pltpu.VMEM)] * 4,
-        out_specs=[pl.BlockSpec(memory_space=pltpu.VMEM)] * 4,
-        compiler_params=pltpu.CompilerParams(vmem_limit_bytes=40 << 20),
-        cost_estimate=pl.CostEstimate(flops=10**9, bytes_accessed=5 << 20, transcendentals=0),
-        name="prep",
-    )(routes, weights, x, c)
-
-
 def expert_kernel(
-    s_in, s_gr, wg_h, wu_h, wd_h, ow_h, mix_h, q_h, k_h, v_h, pm_ref, pl_ref, cot_ref,
-    ld_ref, st_ref,
-    x_out, c_out, gg_out, ug_out, act_out, go_out, gq_out, gk_out, gv_out,
-    recv, xs, wg, wu, wd, acc, half_out, ip, far_in, near_in, ret_t, ret_q, res,
-    w_sem, a_send, a_recv, g_send, g_recv, rs_send, rs_recv, t_send, t_recv, r_send, r_recv, o_sem,
+    routes_h, weights_h, x_h, cot_h, ld_h, st_h, wg_h, wu_h, wd_h, ow_h, mix_h, q_h, k_h, v_h,
+    xt_h, c_h, gg_h, ug_h, act_h, go_out, gq_out, gk_out, gv_out,
+    xt_out, act_out, gg_out, ug_out, o_sem, tails, xs, wg, wu, wd, acc, half_out, ip, far_in, near_in, ret_t, ret_q, res,
+    w_sem, a_send, a_recv, l_send, l_recv, g_send, g_recv, rs_send, rs_recv, t_send, t_recv, r_send, r_recv,
     ow, mix, qkv, cum, cum_t, decay, score, logs, gm, gmb, outer, local, part, peer, got,
     ybuf, zbuf, lt_send, lt_recv, d_send, d_recv, b_send, b_recv, sc_send, sc_recv,
     sy_send, sy_recv, sz_send, sz_recv, cbuf,
+    routes, weights, xq, cq, ld_ref, st_ref, sent, sent_left, stacks, pm_ref, pl_ref, e_sem,
+    stack_sem,
 ):
     n_sp, n_tp = lax.axis_size("sp"), lax.axis_size("tp")
     me, tp = lax.axis_index("sp"), lax.axis_index("tp")
@@ -123,6 +64,36 @@
     def slab(k):
         return pl.ds(pl.multiple_of(k * MAIN, MAIN), MAIN)
 
+    def main_slab(k):
+        return pl.ds(pl.multiple_of(k * MAIN + k // (n_sp // 2) * hl, MAIN), MAIN)
+
+    groups = MAIN // LEFT
+
+    mine_cols = at(tp, share)
+    early = [
+        pltpu.make_async_copy(src, dst, e_sem.at[i])
+        for i, (src, dst) in enumerate(
+            (
+                (routes_h, routes), (x_h.at[:, mine_cols], xq), (weights_h, weights),
+                (cot_h.at[:, mine_cols], cq), (ld_h, ld_ref), (st_h, st_ref),
+            )
+        )
+    ]
+    for load in early:
+        load.start()
+    toks = pm_ref.shape[1]
+    stack_loads = [
+        pltpu.make_async_copy(
+            src.at[:, pl.ds(k * share + g * LANES, LANES)],
+            stacks.at[a, pl.ds(g * toks, toks), pl.ds(k * LANES, LANES)],
+            stack_sem.at[a, k * groups + g],
+        )
+        for a, src in enumerate((x_h, cot_h))
+        for k in range(n_tp)
+        for g in range(groups)
+    ]
+    for load in stack_loads:
+        load.start()
     loads = [
         pltpu.make_async_copy(src, dst, w_sem.at[i])
         for i, (src, dst) in enumerate(
@@ -144,19 +115,34 @@
     lax.fori_loop(1, n_sp, greet, 0)
     for k in (nxt, prv):
         pl.semaphore_signal(barrier, inc=1, device_id={"tp": k}, device_id_type=MESH_ID)
+
+    rows_all = pm_ref.shape[0]
+    e = iota((n_sp, toks), 0)
+    early[0].wait()
+    first = routes[0:1, :] == e
+    second = routes[1:2, :] == e
+    chosen = first | second
+    before = (iota((toks, toks), 0) < iota((toks, toks), 1)).astype(F32).astype(BF)
+    ranks = jnp.where(chosen, dot(chosen.astype(F32).astype(BF), before), -1.0).astype(BF)
+    owner = (iota((rows_all, n_sp), 0) // MAIN == iota((rows_all, n_sp), 1)).astype(F32).astype(BF)
+    spread = dot(owner, ranks).astype(jnp.int32)
+    place = iota((rows_all, toks), 0) % MAIN
+    is_main = spread == place
+    is_left = spread == MAIN + place % LEFT
+    pm_ref[...] = is_main.astype(F32).astype(BF)
+    pl_ref[...] = is_left.astype(F32).astype(BF)
+    early[1].wait()
+    sent[0] = dot(pm_ref[...], xq[...]).astype(BF)
     pl.semaphore_wait(barrier, n_sp + 1)
 
-    for a, src in ((0, s_in), (1, s_gr)):
-        landing = recv.at[a, slab(me), at(tp, wide)]
-        pltpu.make_async_copy(src.at[slab(me), :], landing, a_recv.at[a, me // (n_sp // 2)]).start()
-
+    def spread_out(src, landing, send_sem, recv_sem):
         def deliver(i, carry):
             e = lax.rem(me + i, n_sp)
             pltpu.make_async_remote_copy(
                 src_ref=src.at[slab(e), :],
                 dst_ref=landing,
-                send_sem=a_send.at[a],
-                recv_sem=a_recv.at[a, me // (n_sp // 2)],
+                send_sem=send_sem,
+                recv_sem=recv_sem,
                 device_id={"sp": e},
                 device_id_type=MESH_ID,
             ).start()
@@ -164,7 +150,42 @@
 
         lax.fori_loop(1, n_sp, deliver, 0)
 
-    toks = res.shape[0]
+    def dispatch(a):
+        landing = xs.at[a, main_slab(me), at(tp, share)]
+        spread_out(sent.at[a], landing, a_send.at[a], a_recv.at[a, me // (n_sp // 2)])
+        xs[a, main_slab(me), at(tp, share)] = sent[a, slab(me), :]
+
+    def dispatch_left(a):
+        spread_out(sent_left.at[a], tails.at[a, slab(me), :], l_send.at[a], l_recv.at[a])
+        tails[a, slab(me), :] = sent_left[a, slab(me), :]
+
+    dispatch(0)
+    early[2].wait()
+    early[3].wait()
+    w = jnp.where(first, weights[0:1, :], 0.0) + jnp.where(second, weights[1:2, :], 0.0)
+    w_rows = jnp.zeros((rows_all, toks), F32)
+    for _ in range(3):
+        piece = w.astype(BF)
+        w_rows = w_rows + dot(owner, piece)
+        w = w - piece.astype(F32)
+    w_main = jnp.sum(jnp.where(is_main, w_rows, 0.0), axis=1, keepdims=True)
+    w_left = jnp.sum(jnp.where(is_left, w_rows, 0.0), axis=1, keepdims=True)
+    sent[1] = (w_main * dot(pm_ref[...], cq[...])).astype(BF)
+    dispatch(1)
+    row_group = (iota((rows_all, toks), 0) % MAIN) // LEFT
+    p_left = pl_ref[...]
+    p_wide = jnp.concatenate(
+        [jnp.where(row_group == g, p_left, jnp.zeros_like(p_left)) for g in range(groups)], axis=1
+    )
+    for load in stack_loads:
+        load.wait()
+    sent_left[0] = dot(p_wide, stacks[0]).astype(BF)
+    dispatch_left(0)
+    sent_left[1] = (w_left * dot(p_wide, stacks[1])).astype(BF)
+    dispatch_left(1)
+    early[4].wait()
+    early[5].wait()
+
     blk = toks // 2
     pairs = share // LANES
     core, y_at, z_at = lax.rem(me, 2), lax.rem(me // 2, 4), me // 8
@@ -177,17 +198,17 @@
             v = v - p.astype(F32)
         return out
 
-    heads = ld_ref.shape[1]
+    heads = ld_ref.shape[0]
     lane_head = (iota((heads, share), 1) // (share // heads) == iota((heads, share), 0)).astype(
         F32
     ).astype(BF)
     lower = (iota((blk, blk), 0) >= iota((blk, blk), 1)).astype(F32).astype(BF)
     upper = (iota((blk, blk), 0) <= iota((blk, blk), 1)).astype(F32).astype(BF)
     for b in range(2):
-        steps = pieces(ld_ref[b * blk : (b + 1) * blk, :])
-        cum_t[b * heads : (b + 1) * heads, :] = sum(t_dot(p, upper) for p in steps)
+        steps = pieces(ld_ref[:, b * blk : (b + 1) * blk])
+        cum_t[b * heads : (b + 1) * heads, :] = sum(dot(p, upper) for p in steps)
         cum[b * blk : (b + 1) * blk, :] = sum(
-            dot(lower, dot(p, lane_head).astype(BF)) for p in steps
+            dot(lower, t_dot(p, lane_head).astype(BF)) for p in steps
         )
     ends = [cum[(b + 1) * blk - 1 : (b + 1) * blk, :] for b in range(2)]
 
@@ -258,23 +279,22 @@
     pick = (
         qq == ((jj % MAIN) // LEFT) * hl + (jj // MAIN) * LEFT + jj % LEFT
     ).astype(F32).astype(BF)
-    groups = MAIN // LEFT
-
-    def unpack(a, k):
+    def unpack(a):
+        ref = tails.at[a, pl.ds(0, (n_sp - 1) * MAIN), :]
+        pltpu.make_async_copy(ref, ref, l_recv.at[a]).wait()
         for h in range(2):
-            rows = pl.ds(h * hs, hs)
-            xs[a, h * hx : h * hx + hs, at(k, share)] = recv[a, rows, pl.ds(pl.multiple_of(k * wide, LANES), share)]
-            tail = recv[a, rows, pl.ds(pl.multiple_of(k * wide + share, LANES), LANES)]
-            spread = dot(unpick, tail).astype(BF)
-            left = jnp.concatenate([spread[g * hl : (g + 1) * hl] for g in range(groups)], axis=1)
-            xs[a, h * hx + hs : (h + 1) * hx, at(k, share)] = left
+            spread = dot(unpick, tails[a, h * hs : (h + 1) * hs, :]).astype(BF)
+            for k in range(n_tp):
+                for g in range(groups):
+                    lanes = pl.ds(k * share + g * LANES, LANES)
+                    xs[a, h * hx + hs : (h + 1) * hx, lanes] = spread[
+                        g * hl : (g + 1) * hl, k * LANES : (k + 1) * LANES
+                    ]
 
     def piece_in(k, fresh):
-        unpack(0, k)
-
         @pl.loop(0, 2)
         def _(h):
-            rows = pl.ds(pl.multiple_of(h * hx, MAIN), hx)
+            rows = pl.ds(pl.multiple_of(h * hx, MAIN), hs)
             x = xs[0, rows, at(k, share)]
             g = dot(x, wg[at(k, share), :])
             u = dot(x, wu[at(k, share), :])
@@ -285,29 +305,49 @@
                 acc[0, rows, :] += g
                 acc[1, rows, :] += u
 
-    def piece_gr(k, fresh):
-        unpack(1, k)
+    def left_in():
+        unpack(0)
 
         @pl.loop(0, 2)
         def _(h):
-            rows = pl.ds(pl.multiple_of(h * hx, MAIN), hx)
+            rows = pl.ds(pl.multiple_of(h * hx + hs, MAIN), hl)
+            x = xs[0, rows, :]
+            acc[0, rows, :] = dot(x, wg[...])
+            acc[1, rows, :] = dot(x, wu[...])
+
+    def piece_gr(k, fresh):
+        @pl.loop(0, 2)
+        def _(h):
+            rows = pl.ds(pl.multiple_of(h * hx, MAIN), hs)
             d = dot_t(xs[1, rows, at(k, share)], wd[:, at(k, share)])
             if fresh:
                 acc[2, rows, :] = d
             else:
                 acc[2, rows, :] += d
 
+    def left_gr():
+        unpack(1)
+
+        @pl.loop(0, 2)
+        def _(h):
+            rows = pl.ds(pl.multiple_of(h * hx + hs, MAIN), hl)
+            acc[2, rows, :] = dot_t(xs[1, rows, :], wd[...])
+
     rings = [
         ring_copies(
-            lambda h, k, a=a: recv.at[a, pl.ds(h * hs, hs), at(k, wide)],
+            lambda h, k, a=a: xs.at[a, pl.ds(h * hx, hs), at(k, share)],
             g_send.at[a], g_recv.at[a],
         )
         for a in range(2)
     ]
 
     def wait_arrivals(a, h):
-        ref = recv.at[a, pl.ds(h * hs, hs), at(tp, wide)]
-        pltpu.make_async_copy(ref, ref, a_recv.at[a, h]).wait()
+        for inside in range(2):
+
+            @pl.when((me // (n_sp // 2) == h) == (inside == 1))
+            def _():
+                ref = xs.at[a, pl.ds(h * hx, hs - inside * MAIN), at(tp, share)]
+                pltpu.make_async_copy(ref, ref, a_recv.at[a, h]).wait()
 
     def ring_begin(ring, ready):
         ready(0)
@@ -338,8 +378,7 @@
     rings[0][4].wait_recv()
     rings[0][5].wait_recv()
     piece_in(far, False)
-    x_copy = pltpu.make_async_copy(xs.at[0], x_out, o_sem.at[0])
-    x_copy.start()
+    left_in()
 
     step = 2 * MAIN
 
@@ -351,14 +390,12 @@
         logistic = 1.0 / (1.0 + jnp.exp(-sigmoid_sharpness * clamped))
         linear = jnp.clip(up, -clamp_limit, clamp_limit) + 1.0
         swish = clamped * logistic
-        half_out[2, rows, :] = (swish * linear).astype(BF)
+        half_out[rows, :] = (swish * linear).astype(BF)
         slope = logistic + sigmoid_sharpness * swish * (1.0 - logistic)
         acc[0, rows, :] = jnp.where(gate < clamp_limit, linear * slope, 0.0)
         acc[1, rows, :] = jnp.where(jnp.abs(up) < clamp_limit, swish, 0.0)
 
-    act_copy = pltpu.make_async_copy(half_out.at[2], act_out, o_sem.at[1])
-    act_copy.start()
-
+    left_gr()
     ring_relay(rings[1])
     rings[1][1].wait_recv()
     piece_gr(prv, False)
@@ -367,27 +404,20 @@
     rings[1][4].wait_recv()
     rings[1][5].wait_recv()
     piece_gr(far, False)
-    c_copy = pltpu.make_async_copy(xs.at[1], c_out, o_sem.at[2])
-    c_copy.start()
 
     @pl.loop(0, 2 * hx // step)
     def _(i):
         rows = pl.ds(pl.multiple_of(i * step, step), step)
         act_grad = acc[2, rows, :]
-        half_out[0, rows, :] = (act_grad * acc[0, rows, :]).astype(BF)
-        half_out[1, rows, :] = (act_grad * acc[1, rows, :]).astype(BF)
-
-    gg_copy = pltpu.make_async_copy(half_out.at[0], gg_out, o_sem.at[3])
-    ug_copy = pltpu.make_async_copy(half_out.at[1], ug_out, o_sem.at[4])
-    gg_copy.start()
-    ug_copy.start()
+        gg_out[rows, :] = (act_grad * acc[0, rows, :]).astype(BF)
+        ug_out[rows, :] = (act_grad * acc[1, rows, :]).astype(BF)
 
     def expert_part(k, slot):
         @pl.loop(0, 2)
         def _(h):
             rows = pl.ds(pl.multiple_of(h * hx, MAIN), hx)
-            y = dot_t(half_out[0, rows, :], wg[at(k, share), :])
-            y = y + dot_t(half_out[1, rows, :], wu[at(k, share), :])
+            y = dot_t(gg_out[rows, :], wg[at(k, share), :])
+            y = y + dot_t(ug_out[rows, :], wu[at(k, share), :])
             ip[slot, rows, :] = y.astype(BF)
 
     halves = [pl.ds(0, hx), pl.ds(hx, hx)]
@@ -410,6 +440,23 @@
     rs[2].start()
     expert_part(prv, 2)
     rs[3].start()
+
+    @pl.loop(0, n_tp * groups)
+    def _(i):
+        xt_out[at(i, LANES), :] = xs[0, :, at(i, LANES)].T
+
+    @pl.loop(0, hidden // LANES)
+    def _(i):
+        act_out[at(i, LANES), :] = half_out[:, at(i, LANES)].T
+
+    saves = [
+        pltpu.make_async_copy(src, dst, o_sem.at[i])
+        for i, (src, dst) in enumerate(
+            ((xt_out, xt_h), (xs.at[1], c_h), (gg_out, gg_h), (ug_out, ug_h), (act_out, act_h))
+        )
+    ]
+    for save in saves:
+        save.start()
     rs[0].wait_recv()
     ip[1, halves[0], :] = (ip[1, halves[0], :].astype(F32) + far_in[0].astype(F32)).astype(BF)
     rs[4].start()
@@ -455,13 +502,13 @@
 
     p_left = pl_ref[...]
     y = t_dot(pm_ref[...], ret_q[:, :share])
-    tails = ret_q[:, share:]
+    back = ret_q[:, share:]
     group = (iota(p_left.shape, 0) % MAIN) // LEFT
     y = y + jnp.concatenate(
-        [t_dot(jnp.where(group == g, p_left, jnp.zeros_like(p_left)), tails) for g in range(groups)],
+        [t_dot(jnp.where(group == g, p_left, jnp.zeros_like(p_left)), back) for g in range(groups)],
         axis=1,
     )
-    res[:, at(tp, share)] = (cot_ref[:, at(tp, share)].astype(F32) + y).astype(BF)
+    res[:, at(tp, share)] = (cq[...].astype(F32) + y).astype(BF)
     ring = ring_copies(
         lambda h, k: res.at[pl.ds(h * (toks // 2), toks // 2), at(k, share)], r_send, r_recv
     )
@@ -505,16 +552,38 @@
                 ]
         swaps[i].start()
 
+    my_block = me // 2
+
+    def send_plane(i):
+        k = order[i]
+        swaps[i].wait_recv()
+        rows = plane_rows(k)
+        part[core, rows, :] = (
+            part[core, rows, :].astype(F32) + peer[rows, :].astype(F32)
+        ).astype(BF)
+        for j in range(4):
+            zy = k * 4 + lax.rem(y_at + j, 4)
+
+            @pl.when(zy != my_block)
+            def _():
+                sp_copy(
+                    part.at[core, pl.ds(pl.multiple_of(zy * block, block), block), :],
+                    got.at[my_block], b_send.at[0], b_recv.at[0], zy * 2 + core,
+                ).start()
+
     loads[3].wait()
     piece_res(0)
     ring_relay(ring)
     ring[1].wait_recv()
     piece_res(1)
+    send_plane(0)
     ring[2].wait_recv()
     piece_res(2)
+    send_plane(1)
     ring[4].wait_recv()
     ring[5].wait_recv()
     piece_res(3)
+    send_plane(2)
     gmb[...] = gm[...].astype(BF)
 
     half = LANES // 2
@@ -559,27 +628,7 @@
     for copy in y_sends:
         copy.start()
 
-    my_block = me // 2
-
-    def send_plane(i):
-        k = order[i]
-        swaps[i].wait_recv()
-        rows = plane_rows(k)
-        part[core, rows, :] = (
-            part[core, rows, :].astype(F32) + peer[rows, :].astype(F32)
-        ).astype(BF)
-        for j in range(4):
-            zy = k * 4 + lax.rem(y_at + j, 4)
-
-            @pl.when(zy != my_block)
-            def _():
-                sp_copy(
-                    part.at[core, pl.ds(pl.multiple_of(zy * block, block), block), :],
-                    got.at[my_block], b_send.at[0], b_recv.at[0], zy * 2 + core,
-                ).start()
-
-    send_plane(0)
-    send_plane(1)
+    send_plane(3)
     for copy in y_sends:
         copy.wait_recv()
     inside_y = jnp.zeros_like(total)
@@ -603,9 +652,6 @@
         def _():
             copy.start()
 
-    send_plane(2)
-    send_plane(3)
-
     @pl.loop(0, 2 * pairs)
     def _(i):
         rows, cols, b, p = spot(i)
@@ -615,8 +661,15 @@
             wg_ts = (dot_t(g, side(v, hh)) * decay[i * 2 + hh]).astype(BF)
             outs.append((dot(wg_ts, k), t_dot(wg_ts, q), t_dot(score[i * 2 + hh], g)))
         intra = [jnp.where(low_lane, lo, hi) for lo, hi in zip(*outs)]
-        st = st_ref[b, p]
-        full = jnp.concatenate([side(st, 0), side(st, 1)], axis=0)
+        st = [st_ref[b, 2 * p + hh] for hh in range(2)]
+        none = jnp.zeros_like(st[0])
+        full = jnp.concatenate(
+            [
+                jnp.concatenate([st[0], none], axis=1),
+                jnp.concatenate([none, st[1]], axis=1),
+            ],
+            axis=0,
+        )
         carry = dot_t(g, full) * jnp.exp(cum[rows, cols])
         gq_out[rows, cols] = (intra[0] + carry).astype(BF)
         gm[rows, cols] = intra[1]
@@ -674,25 +727,26 @@
             copy.wait_send()
 
     for a in range(2):
-        ref = recv.at[a, others, at(tp, wide)]
-        pltpu.make_async_copy(ref, ref, a_send.at[a]).wait()
+        for ref, sem in ((sent.at[a, others, :], a_send), (sent_left.at[a, others, :], l_send)):
+            pltpu.make_async_copy(ref, ref, sem.at[a]).wait()
         for copy in rings[a]:
             copy.wait_send()
     for copy in rs + ring:
         copy.wait_send()
+    for save in saves:
+        save.wait()
     pltpu.make_async_copy(ret_q.at[others, :], ret_q.at[others, :], t_send.at[0]).wait()
-    for copy in (x_copy, act_copy, c_copy, gg_copy, ug_copy):
-        copy.wait()
 
 
 def expert_call(
-    s_in, s_gr, w_gate, w_up, w_down, w_out, mixer, queries, key_vectors, value_vectors,
-    p_main, p_left, cotangent, log_decay, states,
+    routes, weights, x, cotangent, log_decay, states, w_gate, w_up, w_down, w_out, mixer,
+    queries, key_vectors, value_vectors,
 ):
     n_sp, n_tp = lax.axis_size("sp"), lax.axis_size("tp")
     width, hidden = w_gate.shape
-    rows, wide = s_in.shape
     share = width // n_tp
+    wide = share + LANES
+    rows = n_sp * MAIN
     full = n_sp * (MAIN + LEFT)
     toks = cotangent.shape[0]
     anyspace = pl.BlockSpec(memory_space=pl.ANY)
@@ -701,39 +755,44 @@
     return pl.pallas_call(
         expert_kernel,
         out_shape=(
-            jax.ShapeDtypeStruct((full, width), BF),
+            jax.ShapeDtypeStruct((width, full), BF),
             jax.ShapeDtypeStruct((full, width), BF),
             jax.ShapeDtypeStruct((full, hidden), BF),
             jax.ShapeDtypeStruct((full, hidden), BF),
-            jax.ShapeDtypeStruct((full, hidden), BF),
+            jax.ShapeDtypeStruct((hidden, full), BF),
             jax.ShapeDtypeStruct((width // n_sp, share), F32),
             jax.ShapeDtypeStruct((toks, share), BF),
             jax.ShapeDtypeStruct((toks, share), BF),
             jax.ShapeDtypeStruct((toks, share), BF),
         ),
-        in_specs=[anyspace] * 10 + [vmem] * 5,
+        in_specs=[anyspace] * 14,
         out_specs=[anyspace] * 5 + [vmem] * 4,
         scratch_shapes=[
-            pltpu.VMEM((2, rows, n_tp * wide), BF),
+            pltpu.VMEM((width, full), BF),
+            pltpu.VMEM((hidden, full), BF),
+            pltpu.VMEM((full, hidden), BF),
+            pltpu.VMEM((full, hidden), BF),
+            dma((5,)),
+            pltpu.VMEM((2, rows, n_tp * LANES), BF),
             pltpu.VMEM((2, full, width), BF),
             pltpu.VMEM(w_gate.shape, BF),
             pltpu.VMEM(w_up.shape, BF),
             pltpu.VMEM(w_down.shape, BF),
             pltpu.VMEM((3, full, hidden), F32),
-            pltpu.VMEM((3, full, hidden), BF),
+            pltpu.VMEM((full, hidden), BF),
             pltpu.VMEM((4, full, share), BF),
             pltpu.VMEM((2, full // 2, share), BF),
             pltpu.VMEM((2, full, share), BF),
             pltpu.VMEM((rows, wide), BF),
             pltpu.VMEM((rows, wide), BF),
             pltpu.VMEM((toks, width), BF),
-            dma((8,)), dma((2,)), dma((2, 2)), dma((2, 6)), dma((2, 6)),
-            dma((6,)), dma((6,)), dma((1,)), dma((1,)), dma((6,)), dma((6,)), dma((5,)),
+            dma((8,)), dma((2,)), dma((2, 2)), dma((2,)), dma((2,)), dma((2, 6)), dma((2, 6)),
+            dma((6,)), dma((6,)), dma((1,)), dma((1,)), dma((6,)), dma((6,)),
             pltpu.VMEM(w_out.shape, BF),
             pltpu.VMEM(mixer.shape, BF),
             pltpu.VMEM((3, toks, share), BF),
             pltpu.VMEM((toks, share), F32),
-            pltpu.VMEM((2 * log_decay.shape[1], toks // 2), F32),
+            pltpu.VMEM((2 * log_decay.shape[0], toks // 2), F32),
             pltpu.VMEM((16, toks // 2, toks // 2), F32),
             pltpu.VMEM((16, toks // 2, toks // 2), BF),
             pltpu.VMEM((n_sp, 8, LANES), F32),
@@ -749,22 +808,71 @@
             dma((1,)), dma((1,)), dma((4,)), dma((4,)), dma((1,)), dma((1,)), dma((1,)),
             dma((1,)), dma((3,)), dma((3,)), dma((3,)), dma((3,)),
             pltpu.VMEM((4, 64, LANES), BF),
+            pltpu.VMEM(routes.shape, jnp.int32),
+            pltpu.VMEM(weights.shape, F32),
+            pltpu.VMEM((toks, share), BF),
+            pltpu.VMEM((toks, share), BF),
+            pltpu.VMEM(log_decay.shape, F32),
+            pltpu.VMEM(states.shape, BF),
+            pltpu.VMEM((2, rows, share), BF),
+            pltpu.VMEM((2, rows, n_tp * LANES), BF),
+            pltpu.VMEM((2, MAIN // LEFT * toks, n_tp * LANES), BF),
+            pltpu.VMEM((rows, toks), BF),
+            pltpu.VMEM((rows, toks), BF),
+            dma((6,)),
+            dma((2, 16)),
         ],
         compiler_params=pltpu.CompilerParams(
-            collective_id=0, has_side_effects=True, vmem_limit_bytes=60 << 20
+            collective_id=0, has_side_effects=True, vmem_limit_bytes=62 << 20
         ),
         cost_estimate=pl.CostEstimate(flops=10**10, bytes_accessed=20 << 20, transcendentals=0),
         name="experts",
     )(
-        s_in, s_gr, w_gate, w_up, w_down, w_out, mixer, queries, key_vectors, value_vectors,
-        p_main, p_left, cotangent, log_decay, states,
+        routes, weights, x, cotangent, log_decay, states, w_gate, w_up, w_down, w_out, mixer,
+        queries, key_vectors, value_vectors,
     )
 
 
-def contract_rows(left, right):
-    return lax.dot_general(
-        left, right, (((0,), (0,)), ((), ())), preferred_element_type=jnp.float32
-    )
+def weight_kernel(
+    xt, c, gg, ug, act, go, gq, gk, gv, gate_out, up_out, down_out, go_out, gq_out, gk_out, gv_out
+):
+    gate_out[...] = dot(xt[...], gg[...])
+    up_out[...] = dot(xt[...], ug[...])
+    down_out[...] = dot(act[...], c[...])
+    go_out[...] = go[...]
+    gq_out[...] = gq[...]
+    gk_out[...] = gk[...]
+    gv_out[...] = gv[...]
+
+
+def weight_call(xt, c, gg, ug, act, go, gq, gk, gv, steps):
+    width, rows = xt.shape
+    hidden = gg.shape[1]
+    tile = width // steps
+    slice_in = pl.BlockSpec((rows, tile), lambda i: (0, i))
+    slice_x = pl.BlockSpec((tile, rows), lambda i: (i, 0))
+    whole = pl.BlockSpec((rows, hidden), lambda i: (0, 0))
+    whole_t = pl.BlockSpec((hidden, rows), lambda i: (0, 0))
+    tall = pl.BlockSpec((tile, hidden), lambda i: (i, 0))
+
+    def banded(v):
+        return pl.BlockSpec((v.shape[0] // steps, v.shape[1]), lambda i: (i, 0))
+
+    small = [banded(v) for v in (go, gq, gk, gv)]
+    return pl.pallas_call(
+        weight_kernel,
+        grid=(steps,),
+        out_shape=(
+            jax.ShapeDtypeStruct((width, hidden), F32),
+            jax.ShapeDtypeStruct((width, hidden), F32),
+            jax.ShapeDtypeStruct((hidden, width), F32),
+        )
+        + tuple(jax.ShapeDtypeStruct(v.shape, v.dtype) for v in (go, gq, gk, gv)),
+        in_specs=[slice_x, slice_in, whole, whole, whole_t] + small,
+        out_specs=[tall, tall, pl.BlockSpec((hidden, tile), lambda i: (0, i))] + small,
+        compiler_params=pltpu.CompilerParams(vmem_limit_bytes=62 << 20),
+        name="weights",
+    )(xt, c, gg, ug, act, go, gq, gk, gv)
 
 
 def shards(
@@ -783,22 +891,13 @@
     log_decay,
     block_states,
 ):
-    s_in, s_gr, p_main, p_left = prep(
-        routes.T, route_weights.T, moe_input, cotangent, lax.axis_size("sp")
+    outs = expert_call(
+        routes.T, route_weights.T, moe_input, cotangent, log_decay.T, block_states,
+        gate_weight[0], up_weight[0], down_weight[0], out_weight, mixer_output,
+        queries, key_vectors, value_vectors,
     )
-    blocks, heads, dim, _ = block_states.shape
-    states = block_states.reshape(blocks, heads // 2, 2, dim, dim)
-    states = jnp.swapaxes(states, 2, 3).reshape(blocks, heads // 2, dim, 2 * dim)
-    rows, row_grads, gate_grad, up_grad, activation, grad_out, grad_queries, grad_keys, grad_values = (
-        expert_call(
-            s_in, s_gr, gate_weight[0], up_weight[0], down_weight[0], out_weight, mixer_output,
-            queries, key_vectors, value_vectors, p_main, p_left, cotangent, log_decay, states,
-        )
-    )
-    grad_gate = contract_rows(rows, gate_grad)[None]
-    grad_up = contract_rows(rows, up_grad)[None]
-    grad_down = contract_rows(activation, row_grads)[None]
-    return (grad_gate, grad_up, grad_down, grad_out, grad_queries, grad_keys, grad_values)
+    grads = weight_call(*outs, steps=WEIGHT_STEPS)
+    return tuple(g[None] for g in grads[:3]) + tuple(grads[3:])
 
 
 def solution(mesh):

time: 171 us -> 139 us (0.81)
  matrix products: 13.6 us -> 0 us
  local copies, waits for them, and re-layouts: 13.2 us -> 0 us
  Pallas kernels: 143 us -> 138 us
    dot_general x3 -> x0, matrix products: 13.6 us -> none  [contract_rows(): lax.dot_general(left, right, (((0,), (0,)), ((), ())), preferred_element_...]
    unnamed x37 -> x0, local copies, waits for them, and re-layouts: 11.2 us -> none
    pallas_call x2, Pallas kernels: 143 us -> 138 us  [the longest x1 126 us: expert_call(): pl.pallas_call(expert_kernel, out_shape=(jax.ShapeDtypeStruct((width, ful...]
    reshape x2 -> x0, local copies, waits for them, and re-layouts: 2.03 us -> none  [the longest x1 1.22 us: shards(): states = block_states.reshape(blocks, heads // 2, 2, dim, dim)]
where the time goes in v2:
time: 139 us
  Pallas kernels  138 us (99%)
    pallas_call x1, Pallas kernels, expert_call(): pl.pallas_call(expert_kernel, out_shape=(jax.ShapeDtypeStruct((width, ful...  126 us
    pallas_call x1, Pallas kernels, weight_call(): pl.pallas_call(weight_kernel, grid=(steps,), out_shape=(jax.ShapeDtypeStr...  12 us

profile of v2, /device:TPU:5, one launch (start us, length us, event | category | flops | bytes accessed | tf_op | source)
XLA Modules:
  0.0 139.1 jit_solution(3325833483096532545)
XLA Ops:
  0.6 126.4 %experts.1 = (bf16[2048,640]{1,0:T(8,128)(2,1)}, bf16[640,2048]{1,0:T(8,128)(2,1)}, bf16[640,512]{1,0:T(8,128)(2,1)}, bf16[640,512]{1,0:T(8,128)(2,1)}, bf16[512...) custom-call(s32[2,256]{1,0:T(2,128)} %bitcast.16, ...), custom_call_target="tpu_custom_call" | custom-call | flops 10000000000 | bytes 20971520 | tf_op jit(solution)/shard_map/experts/pallas_call | solution.py:755
  127.1 12.0 %weights.1 = (f32[2048,512]{1,0:T(8,128)}, f32[2048,512]{1,0:T(8,128)}, f32[512,2048]{1,0:T(8,128)}, f32[64,512]{1,0:T(8,128)}, bf16[256,512]{1,0:T(8,128)(2,1)}...) custom-call(bf16[2048,640]{1,0:T(8,128)(2,1)} %get-tuple-element.23.xt, bf16[640,2048]{1,0:T(8,128)(2,1)} %get-tuple-element.24.c, ...), custom_call_target="tpu_custom_call" | custom-call | tf_op jit(solution)/shard_map/weights/pallas_call | solution.py:862

commit v3 on v2

--- a/solution.py
+++ b/solution.py
@@ -6,7 +6,7 @@
 from jax.experimental.pallas import tpu as pltpu
 
 SP = "sp"
-WEIGHT_STEPS = 8
+WEIGHT_STEPS = 4
 
 
 clamp_limit = 7.0
@@ -291,53 +291,42 @@
                         g * hl : (g + 1) * hl, k * LANES : (k + 1) * LANES
                     ]
 
-    def piece_in(k, fresh):
-        @pl.loop(0, 2)
-        def _(h):
-            rows = pl.ds(pl.multiple_of(h * hx, MAIN), hs)
-            x = xs[0, rows, at(k, share)]
-            g = dot(x, wg[at(k, share), :])
-            u = dot(x, wu[at(k, share), :])
-            if fresh:
-                acc[0, rows, :] = g
-                acc[1, rows, :] = u
-            else:
-                acc[0, rows, :] += g
-                acc[1, rows, :] += u
+    def piece_in(k, h):
+        rows = pl.ds(h * hx, hs)
+        x = xs[0, rows, at(k, share)]
+        for i, w in ((0, wg), (1, wu)):
+            y = dot(x, w[at(k, share), :])
+            acc[i, rows, :] = y if k is tp else acc[i, rows, :] + y
 
     def left_in():
         unpack(0)
-
-        @pl.loop(0, 2)
-        def _(h):
-            rows = pl.ds(pl.multiple_of(h * hx + hs, MAIN), hl)
+        for h in range(2):
+            rows = pl.ds(h * hx + hs, hl)
             x = xs[0, rows, :]
             acc[0, rows, :] = dot(x, wg[...])
             acc[1, rows, :] = dot(x, wu[...])
 
-    def piece_gr(k, fresh):
-        @pl.loop(0, 2)
-        def _(h):
-            rows = pl.ds(pl.multiple_of(h * hx, MAIN), hs)
-            d = dot_t(xs[1, rows, at(k, share)], wd[:, at(k, share)])
-            if fresh:
-                acc[2, rows, :] = d
-            else:
-                acc[2, rows, :] += d
+    def piece_gr(k, h):
+        rows = pl.ds(h * hx, hs)
+        y = dot_t(xs[1, rows, at(k, share)], wd[:, at(k, share)])
+        acc[2, rows, :] = y if k is tp else acc[2, rows, :] + y
 
     def left_gr():
         unpack(1)
-
-        @pl.loop(0, 2)
-        def _(h):
-            rows = pl.ds(pl.multiple_of(h * hx + hs, MAIN), hl)
+        for h in range(2):
+            rows = pl.ds(h * hx + hs, hl)
             acc[2, rows, :] = dot_t(xs[1, rows, :], wd[...])
 
     rings = [
-        ring_copies(
-            lambda h, k, a=a: xs.at[a, pl.ds(h * hx, hs), at(k, share)],
-            g_send.at[a], g_recv.at[a],
-        )
+        [
+            ring_copies(
+                lambda sub, k, a=a, h=h: xs.at[
+                    a, pl.ds(h * hx + sub * (hs // 2), hs // 2), at(k, share)
+                ],
+                g_send.at[a, h], g_recv.at[a, h],
+            )
+            for h in range(2)
+        ]
         for a in range(2)
     ]
 
@@ -349,13 +338,9 @@
                 ref = xs.at[a, pl.ds(h * hx, hs - inside * MAIN), at(tp, share)]
                 pltpu.make_async_copy(ref, ref, a_recv.at[a, h]).wait()
 
-    def ring_begin(ring, ready):
-        ready(0)
-        ring[0].start()
-        ring[2].start()
-        ready(1)
-        ring[3].start()
-        ring[1].start()
+    def ring_begin(ring):
+        for i in (0, 3, 1, 2):
+            ring[i].start()
 
     def ring_relay(ring):
         ring[0].wait_recv()
@@ -363,115 +348,93 @@
         ring[3].wait_recv()
         ring[5].start()
 
-    ring_begin(rings[0], lambda h: wait_arrivals(0, h))
-    loads[0].wait()
-    loads[1].wait()
-    piece_in(tp, True)
-    ring_relay(rings[0])
-    ring_begin(rings[1], lambda h: wait_arrivals(1, h))
-    rings[0][1].wait_recv()
-    piece_in(prv, False)
-    rings[0][2].wait_recv()
-    piece_in(nxt, False)
-    loads[2].wait()
-    piece_gr(tp, True)
-    rings[0][4].wait_recv()
-    rings[0][5].wait_recv()
-    piece_in(far, False)
-    left_in()
+    def begin(a, h):
+        wait_arrivals(a, h)
+        ring_begin(rings[a][h])
+
+    def near_pieces(a, h):
+        rings[a][h][1].wait_recv()
+        (piece_in, piece_gr)[a](prv, h)
+        rings[a][h][2].wait_recv()
+        (piece_in, piece_gr)[a](nxt, h)
+
+    def far_piece(a, h):
+        rings[a][h][4].wait_recv()
+        rings[a][h][5].wait_recv()
+        (piece_in, piece_gr)[a](far, h)
 
     step = 2 * MAIN
 
-    @pl.loop(0, 2 * hx // step)
-    def _(i):
-        rows = pl.ds(pl.multiple_of(i * step, step), step)
-        gate, up = acc[0, rows, :], acc[1, rows, :]
-        clamped = jnp.minimum(gate, clamp_limit)
-        logistic = 1.0 / (1.0 + jnp.exp(-sigmoid_sharpness * clamped))
-        linear = jnp.clip(up, -clamp_limit, clamp_limit) + 1.0
-        swish = clamped * logistic
-        half_out[rows, :] = (swish * linear).astype(BF)
-        slope = logistic + sigmoid_sharpness * swish * (1.0 - logistic)
-        acc[0, rows, :] = jnp.where(gate < clamp_limit, linear * slope, 0.0)
-        acc[1, rows, :] = jnp.where(jnp.abs(up) < clamp_limit, swish, 0.0)
-
-    left_gr()
-    ring_relay(rings[1])
-    rings[1][1].wait_recv()
-    piece_gr(prv, False)
-    rings[1][2].wait_recv()
-    piece_gr(nxt, False)
-    rings[1][4].wait_recv()
-    rings[1][5].wait_recv()
-    piece_gr(far, False)
-
-    @pl.loop(0, 2 * hx // step)
-    def _(i):
-        rows = pl.ds(pl.multiple_of(i * step, step), step)
-        act_grad = acc[2, rows, :]
-        gg_out[rows, :] = (act_grad * acc[0, rows, :]).astype(BF)
-        ug_out[rows, :] = (act_grad * acc[1, rows, :]).astype(BF)
-
-    def expert_part(k, slot):
-        @pl.loop(0, 2)
-        def _(h):
-            rows = pl.ds(pl.multiple_of(h * hx, MAIN), hx)
-            y = dot_t(gg_out[rows, :], wg[at(k, share), :])
-            y = y + dot_t(ug_out[rows, :], wu[at(k, share), :])
-            ip[slot, rows, :] = y.astype(BF)
-
-    halves = [pl.ds(0, hx), pl.ds(hx, hx)]
-
-    def rs_copy(src, dst, i, k):
-        return tp_copy(src, dst, rs_send, rs_recv, i, k)
-
-    rs = [
-        rs_copy(ip.at[0, halves[0]], far_in.at[0], 0, nxt),
-        rs_copy(ip.at[0, halves[1]], far_in.at[1], 1, prv),
-        rs_copy(ip.at[1, halves[1]], near_in.at[0, halves[1]], 2, nxt),
-        rs_copy(ip.at[2, halves[0]], near_in.at[1, halves[0]], 3, prv),
-        rs_copy(ip.at[1, halves[0]], near_in.at[0, halves[0]], 4, nxt),
-        rs_copy(ip.at[2, halves[1]], near_in.at[1, halves[1]], 5, prv),
-    ]
-    expert_part(far, 0)
-    rs[0].start()
-    rs[1].start()
-    expert_part(nxt, 1)
-    rs[2].start()
-    expert_part(prv, 2)
-    rs[3].start()
-
-    @pl.loop(0, n_tp * groups)
-    def _(i):
-        xt_out[at(i, LANES), :] = xs[0, :, at(i, LANES)].T
-
-    @pl.loop(0, hidden // LANES)
-    def _(i):
-        act_out[at(i, LANES), :] = half_out[:, at(i, LANES)].T
-
-    saves = [
-        pltpu.make_async_copy(src, dst, o_sem.at[i])
-        for i, (src, dst) in enumerate(
-            ((xt_out, xt_h), (xs.at[1], c_h), (gg_out, gg_h), (ug_out, ug_h), (act_out, act_h))
-        )
-    ]
-    for save in saves:
-        save.start()
-    rs[0].wait_recv()
-    ip[1, halves[0], :] = (ip[1, halves[0], :].astype(F32) + far_in[0].astype(F32)).astype(BF)
-    rs[4].start()
-    rs[1].wait_recv()
-    ip[2, halves[1], :] = (ip[2, halves[1], :].astype(F32) + far_in[1].astype(F32)).astype(BF)
-    rs[5].start()
-    expert_part(tp, 3)
-
-    for h in range(2):
-        rs[(4, 2)[h]].wait_recv()
-        rs[(3, 5)[h]].wait_recv()
+    def forward_half(h):
+        @pl.loop(0, hx // step)
+        def _(i):
+            rows = pl.ds(pl.multiple_of(h * hx + i * step, step), step)
+            gate, up = acc[0, rows, :], acc[1, rows, :]
+            clamped = jnp.minimum(gate, clamp_limit)
+            logistic = 1.0 / (1.0 + jnp.exp(-sigmoid_sharpness * clamped))
+            linear = jnp.clip(up, -clamp_limit, clamp_limit) + 1.0
+            swish = clamped * logistic
+            half_out[rows, :] = (swish * linear).astype(BF)
+            slope = logistic + sigmoid_sharpness * swish * (1.0 - logistic)
+            acc[0, rows, :] = jnp.where(gate < clamp_limit, linear * slope, 0.0)
+            acc[1, rows, :] = jnp.where(jnp.abs(up) < clamp_limit, swish, 0.0)
+
+    def backward_half(h):
+        @pl.loop(0, hx // step)
+        def _(i):
+            rows = pl.ds(pl.multiple_of(h * hx + i * step, step), step)
+            act_grad = acc[2, rows, :]
+            gg_out[rows, :] = (act_grad * acc[0, rows, :]).astype(BF)
+            ug_out[rows, :] = (act_grad * acc[1, rows, :]).astype(BF)
+
+    def expert_part(k, slot, h):
+        rows = pl.ds(h * hx, hx)
+        y = dot_t(gg_out[rows, :], wg[at(k, share), :])
+        y = y + dot_t(ug_out[rows, :], wu[at(k, share), :])
+        ip[slot, rows, :] = y.astype(BF)
+
+    def sums(h):
+        subs = [pl.ds(h * hx + sub * (hx // 2), hx // 2) for sub in range(2)]
+
+        def rs_copy(src, dst, i, k):
+            return tp_copy(src, dst, rs_send.at[h], rs_recv.at[h], i, k)
+
+        return subs, [
+            rs_copy(ip.at[0, subs[0]], far_in.at[h, 0], 0, nxt),
+            rs_copy(ip.at[0, subs[1]], far_in.at[h, 1], 1, prv),
+            rs_copy(ip.at[1, subs[1]], near_in.at[0, subs[1]], 2, nxt),
+            rs_copy(ip.at[2, subs[0]], near_in.at[1, subs[0]], 3, prv),
+            rs_copy(ip.at[1, subs[0]], near_in.at[0, subs[0]], 4, nxt),
+            rs_copy(ip.at[2, subs[1]], near_in.at[1, subs[1]], 5, prv),
+        ]
+
+    reduces = [sums(h) for h in range(2)]
+
+    def parts(h):
+        for slot, k in enumerate((far, nxt, prv)):
+            expert_part(k, slot, h)
+
+    def send_parts(h):
+        for copy in reduces[h][1][:4]:
+            copy.start()
+
+    def augment(h):
+        subs, rs = reduces[h]
+        for i in range(2):
+            rs[i].wait_recv()
+            ip[1 + i, subs[i], :] = (
+                ip[1 + i, subs[i], :].astype(F32) + far_in[h, i].astype(F32)
+            ).astype(BF)
+            rs[4 + i].start()
+
+    def finish(h):
+        for i in range(2, 6):
+            reduces[h][1][i].wait_recv()
+        rows = pl.ds(h * hx, hx)
         total = (
-            ip[3, halves[h], :].astype(F32)
-            + near_in[0, halves[h], :].astype(F32)
-            + near_in[1, halves[h], :].astype(F32)
+            ip[3, rows, :].astype(F32)
+            + near_in[0, rows, :].astype(F32)
+            + near_in[1, rows, :].astype(F32)
         ).astype(BF)
         ret_t[h * hs : (h + 1) * hs, :share] = total[:hs]
         stacked = jnp.concatenate(
@@ -496,6 +459,64 @@
             return carry
 
         lax.fori_loop(0, n_sp // 2, give_back, 0)
+
+    begin(0, 0)
+    loads[0].wait()
+    loads[1].wait()
+    piece_in(tp, 0)
+    ring_relay(rings[0][0])
+    begin(1, 0)
+    loads[2].wait()
+    piece_gr(tp, 0)
+    near_pieces(0, 0)
+    ring_relay(rings[1][0])
+    begin(0, 1)
+    far_piece(0, 0)
+    piece_in(tp, 1)
+    left_in()
+    forward_half(0)
+    ring_relay(rings[0][1])
+    begin(1, 1)
+    near_pieces(1, 0)
+    left_gr()
+    far_piece(1, 0)
+    backward_half(0)
+    parts(0)
+    ring_relay(rings[1][1])
+    send_parts(0)
+    piece_gr(tp, 1)
+    near_pieces(0, 1)
+    far_piece(0, 1)
+    forward_half(1)
+    expert_part(tp, 3, 0)
+    near_pieces(1, 1)
+    far_piece(1, 1)
+    backward_half(1)
+    parts(1)
+    augment(0)
+    send_parts(1)
+    expert_part(tp, 3, 1)
+
+    @pl.loop(0, hidden // LANES)
+    def _(i):
+        act_out[at(i, LANES), :] = half_out[:, at(i, LANES)].T
+
+    finish(0)
+
+    @pl.loop(0, n_tp * groups)
+    def _(i):
+        xt_out[at(i, LANES), :] = xs[0, :, at(i, LANES)].T
+
+    augment(1)
+    saves = [
+        pltpu.make_async_copy(src, dst, o_sem.at[i])
+        for i, (src, dst) in enumerate(
+            ((xt_out, xt_h), (xs.at[1], c_h), (gg_out, gg_h), (ug_out, ug_h), (act_out, act_h))
+        )
+    ]
+    for save in saves:
+        save.start()
+    finish(1)
     ret_q[slab(me), :] = ret_t[slab(me), :]
     others = pl.ds(0, (n_sp - 1) * MAIN)
     pltpu.make_async_copy(ret_q.at[others, :], ret_q.at[others, :], t_recv.at[0]).wait()
@@ -512,7 +533,7 @@
     ring = ring_copies(
         lambda h, k: res.at[pl.ds(h * (toks // 2), toks // 2), at(k, share)], r_send, r_recv
     )
-    ring_begin(ring, lambda h: None)
+    ring_begin(ring)
     block = share // (2 * pairs)
     plane = pairs * block
     partner = me + 1 - 2 * core
@@ -536,14 +557,14 @@
         for i, k in enumerate(order)
     ]
 
-    def piece_res(i):
+    def piece_mix(i):
+        k = order[i]
+        y = dot(res[:, at(k, share)], ow[at(k, share), :])
+        gm[...] = y if i == 0 else gm[...] + y
+
+    def piece_out(i):
         k = order[i]
         r = res[:, at(k, share)]
-        y = dot(r, ow[at(k, share), :])
-        if i == 0:
-            gm[...] = y
-        else:
-            gm[...] += y
         for j in range(pairs):
             g = t_dot(r[:, j * LANES : (j + 1) * LANES], mix[...]).astype(BF)
             for c in range(2):
@@ -551,6 +572,10 @@
                     c * block : (c + 1) * block
                 ]
         swaps[i].start()
+
+    def piece_res(i):
+        piece_out(i)
+        piece_mix(i)
 
     my_block = me // 2
 
@@ -574,16 +599,15 @@
     loads[3].wait()
     piece_res(0)
     ring_relay(ring)
+    send_plane(0)
     ring[1].wait_recv()
     piece_res(1)
-    send_plane(0)
     ring[2].wait_recv()
     piece_res(2)
     send_plane(1)
     ring[4].wait_recv()
     ring[5].wait_recv()
-    piece_res(3)
-    send_plane(2)
+    piece_mix(3)
     gmb[...] = gm[...].astype(BF)
 
     half = LANES // 2
@@ -603,6 +627,8 @@
     local[0] = total.astype(BF)
     swap_state = sp_copy(local.at[0], cbuf, sc_send.at[0], sc_recv.at[0], partner)
     swap_state.start()
+    send_plane(2)
+    piece_out(3)
     tiles = pl.ds(0, n_sp - 1)
     pltpu.make_async_copy(logs.at[tiles], logs.at[tiles], lt_recv.at[0]).wait()
 
@@ -729,9 +755,9 @@
     for a in range(2):
         for ref, sem in ((sent.at[a, others, :], a_send), (sent_left.at[a, others, :], l_send)):
             pltpu.make_async_copy(ref, ref, sem.at[a]).wait()
-        for copy in rings[a]:
+        for copy in rings[a][0] + rings[a][1]:
             copy.wait_send()
-    for copy in rs + ring:
+    for copy in reduces[0][1] + reduces[1][1] + ring:
         copy.wait_send()
     for save in saves:
         save.wait()
@@ -781,13 +807,13 @@
             pltpu.VMEM((3, full, hidden), F32),
             pltpu.VMEM((full, hidden), BF),
             pltpu.VMEM((4, full, share), BF),
-            pltpu.VMEM((2, full // 2, share), BF),
+            pltpu.VMEM((2, 2, full // 4, share), BF),
             pltpu.VMEM((2, full, share), BF),
             pltpu.VMEM((rows, wide), BF),
             pltpu.VMEM((rows, wide), BF),
             pltpu.VMEM((toks, width), BF),
-            dma((8,)), dma((2,)), dma((2, 2)), dma((2,)), dma((2,)), dma((2, 6)), dma((2, 6)),
-            dma((6,)), dma((6,)), dma((1,)), dma((1,)), dma((6,)), dma((6,)),
+            dma((8,)), dma((2,)), dma((2, 2)), dma((2,)), dma((2,)), dma((2, 2, 6)), dma((2, 2, 6)),
+            dma((2, 6)), dma((2, 6)), dma((1,)), dma((1,)), dma((6,)), dma((6,)),
             pltpu.VMEM(w_out.shape, BF),
             pltpu.VMEM(mixer.shape, BF),
             pltpu.VMEM((3, toks, share), BF),

time: 139 us -> 138 us (level); the launches traced: 139 us -> 137 us
  Pallas kernels: 138 us -> 136 us
where the time goes in v3:
time: 138 us; the launch traced here: 137 us
  Pallas kernels  136 us (99%)
    pallas_call x1, Pallas kernels, expert_call(): pl.pallas_call(expert_kernel, out_shape=(jax.ShapeDtypeStruct((width, ful...  125 us
    pallas_call x1, Pallas kernels, weight_call(): pl.pallas_call(weight_kernel, grid=(steps,), out_shape=(jax.ShapeDtypeStr...  10.7 us

profile of v3, /device:TPU:5, one launch (start us, length us, event | category | flops | bytes accessed | tf_op | source)
XLA Modules:
  0.0 136.6 jit_solution(3573508220621716626)
XLA Ops:
  0.6 125.1 %experts.1 = (bf16[2048,640]{1,0:T(8,128)(2,1)}, bf16[640,2048]{1,0:T(8,128)(2,1)}, bf16[640,512]{1,0:T(8,128)(2,1)}, bf16[640,512]{1,0:T(8,128)(2,1)}, bf16[512...) custom-call(s32[2,256]{1,0:T(2,128)} %bitcast.16, ...), custom_call_target="tpu_custom_call" | custom-call | flops 10000000000 | bytes 20971520 | tf_op jit(solution)/shard_map/experts/pallas_call | solution.py:781
  125.7 10.7 %weights.1 = (f32[2048,512]{1,0:T(8,128)}, f32[2048,512]{1,0:T(8,128)}, f32[512,2048]{1,0:T(8,128)}, f32[64,512]{1,0:T(8,128)}, bf16[256,512]{1,0:T(8,128)(2,1)}...) custom-call(bf16[2048,640]{1,0:T(8,128)(2,1)} %get-tuple-element.23.xt, bf16[640,2048]{1,0:T(8,128)(2,1)} %get-tuple-element.24.c, ...), custom_call_target="tpu_custom_call" | custom-call | tf_op jit(solution)/shard_map/weights/pallas_call | solution.py:888

commit v4 on v3

--- a/solution.py
+++ b/solution.py
@@ -599,9 +599,9 @@
     loads[3].wait()
     piece_res(0)
     ring_relay(ring)
-    send_plane(0)
     ring[1].wait_recv()
     piece_res(1)
+    send_plane(0)
     ring[2].wait_recv()
     piece_res(2)
     send_plane(1)
@@ -627,7 +627,6 @@
     local[0] = total.astype(BF)
     swap_state = sp_copy(local.at[0], cbuf, sc_send.at[0], sc_recv.at[0], partner)
     swap_state.start()
-    send_plane(2)
     piece_out(3)
     tiles = pl.ds(0, n_sp - 1)
     pltpu.make_async_copy(logs.at[tiles], logs.at[tiles], lt_recv.at[0]).wait()
@@ -653,6 +652,7 @@
     ]
     for copy in y_sends:
         copy.start()
+    send_plane(2)
 
     send_plane(3)
     for copy in y_sends:

time: 138 us -> 132 us (0.957)
  Pallas kernels: 136 us -> 130 us
    pallas_call x1, Pallas kernels: 125 us -> 120 us  [expert_call(): pl.pallas_call(expert_kernel, out_shape=(jax.ShapeDtypeStruct((width, ful...]
where the time goes in v4:
time: 132 us; the launch traced here: 131 us
  Pallas kernels  130 us (98%)
    pallas_call x1, Pallas kernels, expert_call(): pl.pallas_call(expert_kernel, out_shape=(jax.ShapeDtypeStruct((width, ful...  120 us
    pallas_call x1, Pallas kernels, weight_call(): pl.pallas_call(weight_kernel, grid=(steps,), out_shape=(jax.ShapeDtypeStr...  10.7 us

profile of v4, /device:TPU:5, one launch (start us, length us, event | category | flops | bytes accessed | tf_op | source)
XLA Modules:
  0.0 131.2 jit_solution(13028424760669278616)
XLA Ops:
  0.6 119.7 %experts.1 = (bf16[2048,640]{1,0:T(8,128)(2,1)}, bf16[640,2048]{1,0:T(8,128)(2,1)}, bf16[640,512]{1,0:T(8,128)(2,1)}, bf16[640,512]{1,0:T(8,128)(2,1)}, bf16[512...) custom-call(s32[2,256]{1,0:T(2,128)} %bitcast.16, ...), custom_call_target="tpu_custom_call" | custom-call | flops 10000000000 | bytes 20971520 | tf_op jit(solution)/shard_map/experts/pallas_call | solution.py:781
  120.3 10.7 %weights.1 = (f32[2048,512]{1,0:T(8,128)}, f32[2048,512]{1,0:T(8,128)}, f32[512,2048]{1,0:T(8,128)}, f32[64,512]{1,0:T(8,128)}, bf16[256,512]{1,0:T(8,128)(2,1)}...) custom-call(bf16[2048,640]{1,0:T(8,128)(2,1)} %get-tuple-element.23.xt, bf16[640,2048]{1,0:T(8,128)(2,1)} %get-tuple-element.24.c, ...), custom_call_target="tpu_custom_call" | custom-call | tf_op jit(solution)/shard_map/weights/pallas_call | solution.py:888

commit v5 on v4

--- a/solution.py
+++ b/solution.py
@@ -6,7 +6,7 @@
 from jax.experimental.pallas import tpu as pltpu
 
 SP = "sp"
-WEIGHT_STEPS = 4
+WEIGHT_STEPS = 2
 
 
 clamp_limit = 7.0

time: 132 us -> 132 us (level)
  no operation moved by 1% of the time
where the time goes in v5:
time: 132 us; the launch traced here: 131 us
  Pallas kernels  130 us (98%)
    pallas_call x1, Pallas kernels, expert_call(): pl.pallas_call(expert_kernel, out_shape=(jax.ShapeDtypeStruct((width, ful...  120 us
    pallas_call x1, Pallas kernels, weight_call(): pl.pallas_call(weight_kernel, grid=(steps,), out_shape=(jax.ShapeDtypeStr...  10.5 us

profile of v5, /device:TPU:5, one launch (start us, length us, event | category | flops | bytes accessed | tf_op | source)
XLA Modules:
  0.0 131.0 jit_solution(8351308418938994057)
XLA Ops:
  0.6 119.7 %experts.1 = (bf16[2048,640]{1,0:T(8,128)(2,1)}, bf16[640,2048]{1,0:T(8,128)(2,1)}, bf16[640,512]{1,0:T(8,128)(2,1)}, bf16[640,512]{1,0:T(8,128)(2,1)}, bf16[512...) custom-call(s32[2,256]{1,0:T(2,128)} %bitcast.16, ...), custom_call_target="tpu_custom_call" | custom-call | flops 10000000000 | bytes 20971520 | tf_op jit(solution)/shard_map/experts/pallas_call | solution.py:781
  120.3 10.5 %weights.1 = (f32[2048,512]{1,0:T(8,128)}, f32[2048,512]{1,0:T(8,128)}, f32[512,2048]{1,0:T(8,128)}, f32[64,512]{1,0:T(8,128)}, bf16[256,512]{1,0:T(8,128)(2,1)}...) custom-call(bf16[2048,640]{1,0:T(8,128)(2,1)} %get-tuple-element.23.xt, bf16[640,2048]{1,0:T(8,128)(2,1)} %get-tuple-element.24.c, ...), custom_call_target="tpu_custom_call" | custom-call | tf_op jit(solution)/shard_map/weights/pallas_call | solution.py:888
